TPU v7x, 512 devices: a whole 4x8x8 slice. The times are simulated.
512 devices in a mesh: sp: 64 (over z, y), fs: 4 (over x), tp: 2 (over core).
Axes of the slice: x: 4, y: 8, z: 8, core: 2. Of those that a mesh axis runs over, the one named last changes fastest.
Arguments:
- tokens: bfloat16 [32768, 2048], P(('fs', 'sp')), parts along dimension 0, may hold values from -6 to 6
- norm_gain: bfloat16 [2048], replicated, may hold values from 0.099609375 to 1.8984375
- query_down: bfloat16 [2048, 512], P('sp'), may hold values from -0.125 to 0.125
- query_gain: bfloat16 [512], replicated, may hold values from 0.099609375 to 1.8984375
- latent_down: bfloat16 [2048, 256], replicated, may hold values from -0.125 to 0.125
- latent_gain: bfloat16 [256], replicated, may hold values from 0.099609375 to 1.8984375
- rope_down: bfloat16 [2048, 64], replicated, may hold values from -30 to 30
- query_up: bfloat16 [512, 1536], P(None, 'tp'), may hold values from -0.25 to 0.25
- key_up: bfloat16 [256, 1024], P(None, 'tp'), may hold values from -0.75 to 0.75
- value_up: bfloat16 [256, 1024], P(None, 'tp'), may hold values from -0.375 to 0.375
- glu_value: bfloat16 [2048, 1024], P('sp', 'tp'), may hold values from -0.125 to 0.125
- glu_gate: bfloat16 [2048, 1024], P('sp', 'tp'), may hold values from -0.125 to 0.125
- conv_taps: bfloat16 [31, 1024], P(None, 'tp'), may hold values from -1 to 1
- group_gain: bfloat16 [1024], P('tp'), may hold values from 0.099609375 to 1.8984375
- head_proj: bfloat16 [1024, 2048], P('tp', 'sp'), may hold values from -0.75 to 0.75
- channel_proj: bfloat16 [1024, 2048], P('tp', 'sp'), may hold values from -0.1875 to 0.1875
Outputs:
- mixed_out: bfloat16 [32768, 2048], P(('fs', 'sp'), 'tp'), parts along dimension 0
- log_weight: float32 [8, 32768], P('tp', ('fs', 'sp')), parts along dimension 1
There are 4 independent parts, one for each index of `fs`. A program takes and returns all parts, laid end to end along the dimension named above; an argument that names none is the same for every part. Nothing has to cross between parts.
All inputs are finite; a program needn't handle non-finite values.
Results may differ from a plain program's by a relative error of at most 0.015.
The roundings to bfloat16 on the way count: a program that leaves them out, or rounds other values in their place, can miss the bound.
Values may be sent and summed in bfloat16 or wider, within the bound.
A program may use at most 128 MiB of HBM per device.

v0:
```python
import jax
import jax.numpy as jnp
from jax import lax
from jax.sharding import PartitionSpec as P

NOPE = 128
ROPE = 64
VDIM = 128
KVR = 256
CH = 1024
GROUPS = 8
GRID_W = 64


norm_eps = 1e-06
rope_base = 10000.0
far_below = -1e30


def in_one_piece(arrays, axis, dim, along):
    widths = [a.shape[along] for a in arrays]
    both = jnp.concatenate(arrays, axis=along)
    result = lax.all_gather(both, axis, axis=dim, tiled=True)
    return tuple(jnp.split(result, [sum(widths[:k]) for k in range(1, len(widths))], axis=along))


def padded_2(block, sides, width):
    for axis, dim in sides:
        count = lax.axis_size(axis)
        forward = [(i, i + 1) for i in range(count - 1)]
        backward = [(target, source) for source, target in forward]
        low = lax.ppermute(
            lax.slice_in_dim(block, block.shape[dim] - width, None, axis=dim), axis, forward
        )
        high = lax.ppermute(lax.slice_in_dim(block, 0, width, axis=dim), axis, backward)
        block = jnp.concatenate([low, block, high], axis=dim)
    return block


def split_up(shard, dim, length):
    before, after = (shard.shape[:dim], shard.shape[dim + 1 :])
    return jnp.moveaxis(shard.reshape(*before, length, -1, *after), dim, 0)


def sent_and_summed(shard, axis, dim):
    tiles = split_up(shard, dim, lax.axis_size(axis))
    arrived = lax.all_to_all(tiles, axis, split_axis=0, concat_axis=0, tiled=True)
    return arrived.astype(jnp.float32).sum(axis=0)


def rms_scale(values, scale_gain):
    inv_rms = lax.rsqrt(jnp.mean(values * values, axis=-1, keepdims=True) + norm_eps)
    return values * inv_rms * scale_gain.astype(jnp.float32)


def angles_for(positions, rope_size):
    quarter = rope_size // 4
    inverse = rope_base ** (-jnp.arange(quarter, dtype=jnp.float32) / quarter)
    grid_row = (positions // GRID_W).astype(jnp.float32)
    grid_col = (positions % GRID_W).astype(jnp.float32)
    return jnp.concatenate([grid_row[:, None] * inverse, grid_col[:, None] * inverse], axis=-1)


def rotate(values, angles):
    half_size = values.shape[-1] // 2
    front_half = values[..., :half_size]
    back_half = values[..., half_size:]
    cosine = jnp.cos(angles)
    sine_part = jnp.sin(angles)
    return jnp.concatenate(
        [front_half * cosine - back_half * sine_part, back_half * cosine + front_half * sine_part],
        axis=-1,
    )


def key_block(normed, latent_down, latent_gain, rope_down, positions):
    latent = jnp.dot(normed, latent_down, preferred_element_type=jnp.float32)
    latent = rms_scale(latent, latent_gain).astype(jnp.bfloat16)
    rope_key = jnp.dot(normed, rope_down, preferred_element_type=jnp.float32)
    rope_key = rotate(rope_key, angles_for(positions, rope_key.shape[-1])).astype(jnp.bfloat16)
    return jnp.concatenate([latent, rope_key], axis=1)


def per_device(
    tokens,
    norm_gain,
    query_down,
    query_gain,
    latent_down,
    latent_gain,
    rope_down,
    query_up,
    key_up,
    value_up,
    glu_value,
    glu_gate,
    conv_taps,
    group_gain,
    head_proj,
    channel_proj,
):
    tok_count = tokens.shape[0]
    reach_rows = conv_taps.shape[0] // 2
    head_count = key_up.shape[1] // NOPE
    normed = rms_scale(tokens.astype(jnp.float32), norm_gain).astype(jnp.bfloat16)
    offsets = lax.axis_index("sp") * tok_count + jnp.arange(tok_count, dtype=jnp.int32)
    blocks = in_one_piece((query_down, glu_value, glu_gate), "sp", 0, 1)
    query_latent = jnp.dot(normed, blocks[0], preferred_element_type=jnp.float32)
    value_in = jnp.dot(normed, blocks[1], preferred_element_type=jnp.float32)
    gate_in = jnp.dot(normed, blocks[2], preferred_element_type=jnp.float32)
    latent_query = rms_scale(query_latent, query_gain).astype(jnp.bfloat16)
    query_all = jnp.dot(latent_query, query_up, preferred_element_type=jnp.float32).reshape(
        tok_count, head_count, NOPE + ROPE
    )
    query_plain = query_all[:, :, :NOPE].astype(jnp.bfloat16)
    query_rope = rotate(query_all[:, :, NOPE:], angles_for(offsets, ROPE)[:, None, :]).astype(
        jnp.bfloat16
    )
    absorbed = jnp.einsum(
        "thd,rhd->htr",
        query_plain,
        key_up.reshape(KVR, head_count, NOPE),
        preferred_element_type=jnp.float32,
    ).astype(jnp.bfloat16)
    queries = jnp.concatenate([absorbed, jnp.transpose(query_rope, (1, 0, 2))], axis=-1)
    score_scale = (NOPE + ROPE) ** (-0.5)
    half_rows = tok_count // lax.axis_size("tp")
    first_row = lax.axis_index("tp") * half_rows
    own_rows = lax.dynamic_slice_in_dim(normed, first_row, half_rows, 0)
    own_positions = lax.dynamic_slice_in_dim(offsets, first_row, half_rows, 0)
    own_keys = key_block(own_rows, latent_down, latent_gain, rope_down, own_positions)
    block_keys = lax.all_gather(own_keys, ("sp", "tp"), axis=0, tiled=True)
    row_max = jnp.full((head_count, tok_count), far_below, jnp.float32)
    scores = (
        jnp.einsum("hqc,kc->hqk", queries, block_keys, preferred_element_type=jnp.float32)
        * score_scale
    )
    new_max = jnp.maximum(row_max, jnp.max(scores, axis=2))
    weights = jnp.exp(scores - new_max[:, :, None])
    new_sum = jnp.sum(weights, axis=2)
    added = jnp.einsum(
        "hqk,kr->hqr",
        weights.astype(jnp.bfloat16),
        block_keys[:, :KVR],
        preferred_element_type=jnp.float32,
    )
    gated_rows = (value_in * jax.nn.sigmoid(gate_in)).astype(jnp.bfloat16)
    padded = padded_2(gated_rows, (("sp", 0),), reach_rows)
    filtered = padded[0:tok_count].astype(jnp.float32) * conv_taps[0].astype(jnp.float32)
    for tap_index in range(1, conv_taps.shape[0]):
        filtered = filtered + padded[tap_index : tap_index + tok_count].astype(
            jnp.float32
        ) * conv_taps[tap_index].astype(jnp.float32)
    grouped = filtered.reshape(tok_count, -1, CH // GROUPS)
    centred = grouped - jnp.mean(grouped, axis=-1, keepdims=True)
    spread = jnp.mean(centred * centred, axis=-1, keepdims=True)
    normal_groups = (centred * lax.rsqrt(spread + norm_eps)).reshape(tok_count, -1)
    conv_branch = jax.nn.silu(normal_groups * group_gain.astype(jnp.float32)).astype(jnp.bfloat16)
    attended = (added / new_sum[:, :, None]).astype(jnp.bfloat16)
    log_weight = new_max + jnp.log(new_sum)
    head_out = jnp.einsum(
        "htr,rhv->thv",
        attended,
        value_up.reshape(KVR, head_count, VDIM),
        preferred_element_type=jnp.float32,
    )
    head_out = head_out.reshape(tok_count, head_count * VDIM).astype(jnp.bfloat16)
    mixed_in = jnp.concatenate([head_out, conv_branch], axis=1)
    out_weight = jnp.concatenate([head_proj, channel_proj], axis=0)
    partial_terms = jnp.dot(
        mixed_in,
        lax.all_gather(out_weight, "sp", axis=1, tiled=True),
        preferred_element_type=jnp.float32,
    )
    mixed_out = sent_and_summed(partial_terms.astype(jnp.bfloat16), "tp", 1).astype(jnp.bfloat16)
    return (mixed_out, log_weight)


def solution(mesh):
    in_specs = (
        P(("fs", "sp"), None),
        P(),
        P("sp", None),
        P(),
        P(),
        P(),
        P(),
        P(None, "tp"),
        P(None, "tp"),
        P(None, "tp"),
        P("sp", "tp"),
        P("sp", "tp"),
        P(None, "tp"),
        P("tp"),
        P("tp", "sp"),
        P("tp", "sp"),
    )
    out_specs = (P(("fs", "sp"), "tp"), P("tp", ("fs", "sp")))
    return jax.shard_map(
        per_device, mesh=mesh, in_specs=in_specs, out_specs=out_specs, check_vma=False
    )
```

profile of v0, /device:TPU:1, one launch (start us, length us, event | category | flops | bytes accessed | tf_op | source)
XLA Modules:
  0.0 295.6 jit_solution(11499413010207656620)
XLA Ops:
  7.2 1.5 pad_maximum_fusion.2
  8.8 0.7 convert_element_type.239
  9.5 0.7 convert_element_type.232
  10.3 1.2 fusion.32
  11.5 1.2 fusion.34
  12.8 0.4 multiply_reduce_fusion.3
  13.3 1.2 fusion.53
  14.7 0.7 pad_maximum_fusion.4
  15.5 1.4 pad_maximum_fusion.3
  17.0 0.7 convert_element_type.234
  17.7 0.7 convert_element_type.280
  18.7 1.1 copy.70
  19.8 1.0 slice_convert_fusion.31
  20.8 1.0 slice_convert_fusion.32
  21.8 84.6 %all-gather.4.cloned.1.call-done = bf16[2048,1536]{1,0:T(8,128)(2,1)} async-done(((bf16[32,1536]{1,0:T(8,128)(2,1)}), bf16[2048,1536]{1,0:T(8,128)(2,1)}) %all-gather.4.cloned.1.call-update) | async-done | bytes 6291472 | tf_op jit(solution)/shard_map/all_gather | solution.py:23
  106.4 2.1 fusion.26
  108.5 2.1 fusion.29
  110.6 1.9 collective-permute-start
  112.6 1.3 collective-permute-start.1
  113.9 2.1 multiply_reduce_fusion.2
  116.0 0.5 fusion.57
  117.3 76.4 %all-gather.6.cloned.1.call-done = bf16[8192,320]{1,0:T(8,128)(2,1)} async-done(((bf16[64,320]{1,0:T(8,128)(2,1)}), bf16[8192,320]{1,0:T(8,128)(2,1)}) %all-gather.6.cloned.1.call-update) | async-done | bytes 5242896 | tf_op jit(solution)/shard_map/all_gather | solution.py:132
  193.6 10.9 %multiply_reduce_fusion = (f32[4,128]{1,0:T(4,128)S(1)}, f32[4,128,8192]{2,1,0:T(8,128)}) fusion(bf16[8192,320]{1,0:T(8,128)(2,1)} %all-gather.6.cloned.1.call-done, bf16[4,128,64]{2,1,0:T(8,128)(2,1)S(1)} %maximum_bitcast_fusion, bf16[4,128,256]{2,1,0:T(8,128)(2,1)S(1)} %convolution_convert_fusion.1), kind=kOutput, calls=%fused_computation.1 | convolution fusion | flops 2693398016 | bytes 22349824 | tf_op jit(solution)/shard_map/hqc,kc->hqk/dot_general | solution.py:135
  204.5 8.7 %fusion = f32[4,128]{1,0:T(4,128)S(1)} fusion(f32[4,128,8192]{2,1,0:T(8,128)} %get-tuple-element.54, f32[4,128]{1,0:T(4,128)S(1)} %broadcast_maximum_fusion), kind=kLoop, calls=%fused_computation.2 | loop fusion | flops 12582400 | bytes 16781312 | tf_op jit(solution)/shard_map/reduce_sum | solution.py:140
  213.2 9.9 %convolution_convert_fusion.2 = bf16[4,128,128]{1,2,0:T(8,128)(2,1)S(1)} fusion(bf16[256,4,128]{0,2,1:T(8,128)(2,1)S(1)} %bitcast.94, bf16[8192,320]{1,0:T(8,128)(2,1)} %all-gather.6.cloned.1.call-done, f32[4,128,8192]{2,1,0:T(8,128)} %get-tuple-element.54, f32[4,128]{1,0:T(4,128)S(1)} %broadcast_maximum_fusion, f32[4,128]{1,0:T(4,128)S(1)} %fusion), kind=kOutput, calls=%fused_computation.26 | convolution fusion | flops 2193948672 | bytes 21368832 | tf_op jit(solution)/shard_map/htr,rhv->thv/dot_general | solution.py:161
  223.1 0.6 log_add_fusion
  223.8 1.0 multiply_add_fusion
  225.1 0.4 multiply_reduce_fusion.1
  226.0 49.8 %all-gather.8.cloned.1.call-done = bf16[1024,2048]{0,1:T(8,128)(2,1)} async-done(((bf16[1024,32]{0,1:T(8,128)(2,1)}), bf16[1024,2048]{0,1:T(8,128)(2,1)}) %all-gather.8.cloned.1.call-update) | async-done | bytes 4194320 | tf_op jit(solution)/shard_map/all_gather | solution.py:172
  275.9 3.7 %convolution_convert_fusion = bf16[128,2048]{1,0:T(8,128)(2,1)S(1)} fusion(bf16[1024,2048]{0,1:T(8,128)(2,1)} %all-gather.8.cloned.1.call-done, bf16[128,512]{1,0:T(8,128)(2,1)S(1)} %multiply_convert_fusion, bf16[128,512]{1,0:T(8,128)(2,1)S(1)} %copy.64), kind=kOutput, calls=%fused_computation.10 | convolution fusion | flops 537657344 | bytes 4980736 | tf_op jit(solution)/shard_map/dot_general | solution.py:170
  279.6 8.6 %all_to_all.5 = bf16[2,128,1024]{2,1,0:T(8,128)(2,1)S(1)} all-to-all(bf16[2,128,1024]{2,1,0:T(8,128)(2,1)S(1)} %bitcast.89), channel_id=1, replica_groups=mesh['sp'=64,'fs'=4,'tp'=2] {'tp'}, dimensions={0} | all-to-all | bytes 1048576 | tf_op jit(solution)/shard_map/all_to_all | solution.py:47
  288.2 0.8 reduce_sum.72
  (46 shorter events, 2.8 us)
Async XLA Ops:
  7.2 5.6 %copy-start = (bf16[2048,256]{1,0:T(8,128)(2,1)S(1)}, bf16[2048,256]{1,0:T(8,128)(2,1)}, u32[]{:S(2)}) copy-start(bf16[2048,256]{1,0:T(8,128)(2,1)} %param.20) | copy-start | bytes 3145732
  7.2 99.3 %all-gather.4.cloned.1.call-start = ((), (), s32[]{:S(2)}) async-start(), calls=%async_computation.1 | async-start | bytes 6389760 | tf_op jit(solution)/shard_map/all_gather | solution.py:23
  8.8 184.9 %all-gather.6.cloned.1.call-start = ((), (), s32[]{:S(2)}) async-start(), calls=%async_computation.2 | async-start | bytes 6340608 | tf_op jit(solution)/shard_map/all_gather | solution.py:132
  14.6 101.4 %copy-start.1 = (bf16[512,768]{1,0:T(8,128)(2,1)S(1)}, bf16[512,768]{1,0:T(8,128)(2,1)}, u32[]{:S(2)}) copy-start(bf16[512,768]{1,0:T(8,128)(2,1)} %param.23) | copy-start | bytes 2359300
  15.5 260.4 %all-gather.8.cloned.1.call-start = ((), (), s32[]{:S(2)}) async-start(), calls=%async_computation.3 | async-start | bytes 4259840 | tf_op jit(solution)/shard_map/all_gather | solution.py:172
  108.5 8.5 %copy-start.2 = (bf16[256,512]{1,0:T(8,128)(2,1)S(1)}, bf16[256,512]{1,0:T(8,128)(2,1)}, u32[]{:S(2)}) copy-start(bf16[256,512]{1,0:T(8,128)(2,1)} %param.24) | copy-start | bytes 786436
  110.6 113.2 %collective-permute-start = (bf16[15,512]{1,0:T(8,128)(2,1)S(1)}, bf16[15,512]{1,0:T(8,128)(2,1)S(1)}, u32[]{:S(2)}, u32[]{:S(2)}) collective-permute-start(bf16[15,512]{1,0:T(8,128)(2,1)S(1)} %get-tuple-element.8), channel_id=1, source_target_pairs={{0,8},{8,16},{16,24},{24,32},{32,40},{40,48},{48,56},{56,64},{64,7... | collective-permute-start | bytes 46088 | tf_op jit(solution)/shard_map/ppermute | solution.py:32
  112.6 111.3 %collective-permute-start.1 = (bf16[15,512]{1,0:T(8,128)(2,1)S(1)}, bf16[15,512]{1,0:T(8,128)(2,1)S(1)}, u32[]{:S(2)}, u32[]{:S(2)}) collective-permute-start(bf16[15,512]{1,0:T(8,128)(2,1)S(1)} %get-tuple-element.9), channel_id=1, source_target_pairs={{8,0},{16,8},{24,16},{32,24},{40,32},{48,40},{56,48},{64,56},{72,6... | collective-permute-start | bytes 46088 | tf_op jit(solution)/shard_map/ppermute | solution.py:35
Sparse Core Ops, SparseCore 0:
  11.6 94.8 all-gather.3
  109.6 84.0 all-gather.5
  196.7 79.1 all-gather.7
where the time goes:
time: 296 us
  waiting for transfers between devices  211 us (71%)
  matrix products  33.1 us (11%)
  other arithmetic  23.5 us (8%)
  between operations  14 us (5%)
  blocking collectives  8.59 us (3%)
  starting transfers between devices  3.33 us (1%)
    all_gather x1, waiting for transfers between devices, in_one_piece(): result = lax.all_gather(both, axis, axis=dim, tiled=True)  84.6 us
    all_gather x1, waiting for transfers between devices, per_device(): block_keys = lax.all_gather(own_keys, ('sp', 'tp'), axis=0, tiled=True)  76.4 us
    all_gather x1, waiting for transfers between devices, per_device(): lax.all_gather(out_weight, 'sp', axis=1, tiled=True)  49.8 us
    dot_general x1, matrix products, per_device(): jnp.einsum('hqc,kc->hqk', queries, block_keys, preferred_element_type=jnp...  10.9 us
    dot_general x1, matrix products, per_device(): jnp.einsum('htr,rhv->thv', attended, value_up.reshape(KVR, head_count, VD...  9.88 us
    reduce_sum x1, other arithmetic, per_device(): new_sum = jnp.sum(weights, axis=2)  8.7 us
    all_to_all x1, blocking collectives, sent_and_summed(): lax.all_to_all(tiles, axis, split_axis=0, concat_axis=0, tiled=True)  8.59 us
  transfers between devices with their start and end apart: 5, of which 3 were waited for; matrix products, arithmetic and copies ran while one was open for 18% of the time, Pallas kernels for 0%

commit v1 on v0

v1 whole, which is shorter than its diff:
```python
import functools
import math

import jax
import jax.numpy as jnp
import numpy as np
from jax import lax
from jax.experimental import pallas as pl
from jax.experimental.pallas import tpu as pltpu
from jax.sharding import PartitionSpec as P

NOPE = 128
ROPE = 64
VDIM = 128
KVR = 256
GROUP = 128
GRID_W = 64
EPS = 1e-06
BASE = 10000.0
HALO = 16
NX = 4
F32 = jnp.float32
BF16 = jnp.bfloat16
MESH = pl.DeviceIdType.MESH


def dot(a, b):
    return jnp.dot(a, b, preferred_element_type=F32)


def dot_t(a, b):
    return lax.dot_general(a, b, (((1,), (1,)), ((), ())), preferred_element_type=F32)


def rms(values, gain):
    inv = lax.rsqrt(jnp.mean(values * values, axis=-1, keepdims=True) + EPS)
    return values * inv * gain


def swap(v):
    half = v.shape[-1] // 2
    return jnp.concatenate([v[:, half:], v[:, :half]], axis=-1)


class Gather:
    def __init__(self, view, nz, ny, z, y, p_send, p_recv, r_send, r_recv):
        self.view, self.size, self.pos = view, (nz, ny), (z, y)
        self.p_send, self.p_recv, self.r_send, self.r_recv = p_send, p_recv, r_send, r_recv
        self.sent = []

    def device(self, axis, k):
        z, y = (k, self.pos[1]) if axis == 0 else (self.pos[0], k)
        return {"sp": z * self.size[1] + y}

    def first_copy(self, half, d, outgoing):
        axis = 1 - half
        n = self.size[axis]
        me = self.pos[axis]
        source = me if outgoing else lax.rem(me + n - d, n)
        z, y = (source, self.pos[1]) if axis == 0 else (self.pos[0], source)
        ref = self.view.at[z, y, half]
        return pltpu.make_async_remote_copy(
            src_ref=ref,
            dst_ref=ref,
            send_sem=self.p_send.at[half, d - 1],
            recv_sem=self.p_recv.at[half, d - 1],
            device_id=self.device(axis, lax.rem(me + d, n)),
            device_id_type=MESH,
        )

    def start_first(self):
        for half in (0, 1):
            for d in range(1, self.size[1 - half]):
                copy = self.first_copy(half, d, True)
                copy.start()
                self.sent.append(copy)

    def wait_first(self):
        for half in (0, 1):
            for d in range(1, self.size[1 - half]):
                self.first_copy(half, d, False).wait_recv()

    def block(self, half, k, part=None):
        n = self.size[1 - half]
        rows = slice(None) if part is None else pl.ds(part * (n // 2), n // 2)
        return self.view.at[k, rows, 0] if half == 0 else self.view.at[rows, k, 1]

    def steps(self, half):
        return self.size[half] // 2

    def ring_block(self, half, way, s, outgoing):
        n = self.size[half]
        back = s - 1 if outgoing else s
        sign = 1 - 2 * way
        k = lax.rem(self.pos[half] - sign * back + n, n)
        return self.block(half, k, way if s == n // 2 else None)

    def ring_copy(self, half, way, s, outgoing):
        n = self.size[half]
        ref = self.ring_block(half, way, s, outgoing)
        target = lax.rem(self.pos[half] + (1 - 2 * way) + n, n)
        return pltpu.make_async_remote_copy(
            src_ref=ref,
            dst_ref=ref,
            send_sem=self.r_send.at[half, way, s - 1],
            recv_sem=self.r_recv.at[half, way, s - 1],
            device_id=self.device(half, target),
            device_id_type=MESH,
        )

    def start_ring(self, s):
        for half in (0, 1):
            for way in (0, 1):
                copy = self.ring_copy(half, way, s, True)
                copy.start()
                self.sent.append(copy)

    def wait_ring(self, s):
        for half in (0, 1):
            for way in (0, 1):
                self.ring_copy(half, way, s, False).wait_recv()

    def finish(self):
        for copy in self.sent:
            copy.wait_send()


def kernel(
    nz,
    ny,
    tokens,
    norm_gain,
    down_shard,
    query_gain,
    latent_down,
    latent_gain,
    rope_down,
    query_up,
    key_up,
    value_up,
    conv_taps,
    group_gain,
    out_shard,
    inv_freq,
    out,
    log_weight,
    normed4,
    down_all,
    keys_all,
    out_all,
    ql_send,
    ql_recv,
    gated,
    wide,
    conv_send,
    conv_recv,
    queries,
    row_max,
    row_sum,
    acc,
    head_out,
    part_send,
    part_recv,
    local_sem,
    down_p_send,
    down_p_recv,
    down_r_send,
    down_r_recv,
    keys_p_send,
    keys_p_recv,
    keys_r_send,
    keys_r_recv,
    out_p_send,
    out_p_recv,
    out_r_send,
    out_r_recv,
    pair_send,
    pair_recv,
    pair0_send,
    pair0_recv,
    x_send,
    x_recv,
    xp_send,
    xp_recv,
    ql_ssem,
    ql_rsem,
    cv_ssem,
    cv_rsem,
    halo_ssem,
    halo_rsem,
    fin_sem,
):
    sp = lax.axis_index("sp")
    x = lax.axis_index("fs")
    c = lax.axis_index("tp")
    z, y = sp // ny, lax.rem(sp, ny)
    other = 1 - c
    count = tokens.shape[0]
    half_rows = count // 2
    heads = key_up.shape[1] // NOPE

    load_down = pltpu.make_async_copy(down_shard, down_all.at[z, y], local_sem.at[0])
    load_down.start()
    load_out = pltpu.make_async_copy(out_shard, out_all.at[z, y], local_sem.at[1])
    load_out.start()

    barrier = pltpu.get_barrier_semaphore()

    def greet(**where):
        pl.semaphore_signal(barrier, inc=1, device_id=where, device_id_type=MESH)

    for d in range(1, ny):
        greet(sp=z * ny + lax.rem(y + d, ny))
    for d in range(1, nz):
        greet(sp=lax.rem(z + d, nz) * ny + y)
    for d in range(1, NX):
        greet(fs=lax.rem(x + d, NX))
    greet(tp=other)
    has_low = sp > 0
    has_high = sp < nz * ny - 1

    @pl.when(has_low)
    def _():
        greet(sp=sp - 1)

    @pl.when(has_high)
    def _():
        greet(sp=sp + 1)

    gain = norm_gain[...].astype(F32)
    chunk = 32
    for k in range(count // chunk):
        rows = tokens[k * chunk : (k + 1) * chunk, :].astype(F32)
        value = rms(rows, gain).astype(BF16)
        which, first = divmod(k * chunk, half_rows)
        normed4[x, which, first : first + chunk, :] = value

    edges = has_low.astype(jnp.int32) + has_high.astype(jnp.int32)
    pl.semaphore_wait(barrier, (ny - 1) + (nz - 1) + (NX - 1) + 1 + edges)
    load_down.wait()
    load_out.wait()

    g_down = Gather(down_all, nz, ny, z, y, down_p_send, down_p_recv, down_r_send, down_r_recv)
    g_keys = Gather(keys_all.at[c], nz, ny, z, y, keys_p_send, keys_p_recv, keys_r_send, keys_r_recv)
    g_out = Gather(out_all, nz, ny, z, y, out_p_send, out_p_recv, out_r_send, out_r_recv)
    sent = []

    def send(src, dst, ssem, rsem, where):
        copy = pltpu.make_async_remote_copy(
            src_ref=src, dst_ref=dst, send_sem=ssem, recv_sem=rsem, device_id=where, device_id_type=MESH
        )
        copy.start()
        sent.append(copy)

    def arrived(dst, ssem, rsem, where):
        pltpu.make_async_remote_copy(
            src_ref=dst, dst_ref=dst, send_sem=ssem, recv_sem=rsem, device_id=where, device_id_type=MESH
        ).wait_recv()

    g_down.start_first()
    for way in (0, 1):
        mine = normed4.at[x, c]
        where = {"fs": lax.rem(x + (1 - 2 * way) + NX, NX)}
        send(mine, mine, x_send.at[way], x_recv.at[way], where)

    freq = inv_freq[...]
    at_row = lax.broadcasted_iota(jnp.int32, (count, ROPE), 0)
    lane = lax.broadcasted_iota(jnp.int32, (count, ROPE), 1)
    place = at_row + sp * count
    grid_row = (place // GRID_W).astype(F32)
    grid_col = lax.rem(place, GRID_W).astype(F32)
    angles = jnp.where(lax.rem(lane, ROPE // 2) < ROPE // 4, grid_row, grid_col) * freq
    cosine = jnp.cos(angles)
    sine = jnp.sin(angles) * jnp.where(lane < ROPE // 2, -1.0, 1.0)
    wide[0, 0:count, 0:ROPE] = cosine
    wide[1, 0:count, 0:ROPE] = sine

    own = normed4[x, c]
    latent = rms(dot(own, latent_down[...]), latent_gain[...].astype(F32))
    rope_key = dot(own, rope_down[...])
    first = pl.multiple_of(c * half_rows, half_rows)
    rope_key = rope_key * wide[0, pl.ds(first, half_rows), 0:ROPE] + swap(rope_key) * wide[
        1, pl.ds(first, half_rows), 0:ROPE
    ]
    quarter = half_rows // 2
    rope_pair = jnp.concatenate([rope_key[:quarter], rope_key[quarter:]], axis=1).astype(BF16)
    latent = latent.astype(BF16)
    for h in (0, 1):
        lo = h * (quarter // 2)
        hi = lo + quarter // 2
        keys_all[c, z, y, h, :, 0:KVR] = latent[lo:hi]
        keys_all[c, z, y, h, :, KVR : 2 * KVR] = latent[quarter + lo : quarter + hi]
        keys_all[c, z, y, h, :, 2 * KVR :] = rope_pair[lo:hi]

    g_keys.start_first()

    partner = {"tp": other}

    def pair_keys(half, way, s):
        block = g_keys.ring_block(half, way, s, False)
        send(block, block, pair_send.at[half, way, s - 1], pair_recv.at[half, way, s - 1], partner)

    g_down.wait_first()
    g_down.start_ring(1)
    g_keys.wait_first()
    g_keys.start_ring(1)
    own_block = (g_keys.block(0, z), g_keys.block(1, y))
    for half in (0, 1):
        send(own_block[half], own_block[half], pair0_send.at[half], pair0_recv.at[half], partner)

    turn = 1 - 2 * c
    far = lax.rem(x + 2, NX)
    for way in (0, 1):
        src = lax.rem(x - (1 - 2 * way) + NX, NX)
        piece = normed4.at[src, c]
        arrived(piece, x_send.at[way], x_recv.at[way], partner)
        send(piece, piece, xp_send.at[way], xp_recv.at[way], partner)
    onward = normed4.at[lax.rem(x - turn + NX, NX), c]
    send(onward, onward, x_send.at[2], x_recv.at[2], {"fs": lax.rem(x + turn + NX, NX)})

    last = nz // 2
    for s in range(1, last):
        g_down.wait_ring(s)
        g_down.start_ring(s + 1)
        g_keys.wait_ring(s)
        g_keys.start_ring(s + 1)
        for half in (0, 1):
            for way in (0, 1):
                pair_keys(half, way, s)
        if s == 1:
            piece = normed4.at[far, c]
            arrived(piece, x_send.at[2], x_recv.at[2], partner)
            send(piece, piece, xp_send.at[2], xp_recv.at[2], partner)

    g_out.start_first()

    for k in range(3):
        if k < 2:
            src = lax.rem(x - (1 - 2 * k) + NX, NX)
        else:
            src = far
        piece = normed4.at[src, other]
        arrived(piece, xp_send.at[k], xp_recv.at[k], partner)
    g_down.wait_ring(last)

    depth = tokens.shape[1]
    weights = down_all[...].reshape(depth, 3 * GROUP)
    for j in range(NX):
        rows = normed4[j].reshape(count, depth)
        product = dot(rows, weights)
        gate = product[:, GROUP : 2 * GROUP]
        gated[j, HALO : HALO + count, :] = (product[:, :GROUP] * jax.nn.sigmoid(gate)).astype(BF16)
        ql_send[j] = product[:, 2 * GROUP :]
    edge = jnp.zeros((NX, HALO, GROUP), BF16)

    low_src, high_src = gated.at[:, pl.ds(HALO, HALO)], gated.at[:, pl.ds(count, HALO)]
    low_dst, high_dst = gated.at[:, pl.ds(0, HALO)], gated.at[:, pl.ds(HALO + count, HALO)]

    def halo_copy(up):
        src, dst = (high_src, low_dst) if up else (low_src, high_dst)
        k = 0 if up else 1
        return pltpu.make_async_remote_copy(
            src_ref=src,
            dst_ref=dst,
            send_sem=halo_ssem.at[k],
            recv_sem=halo_rsem.at[k],
            device_id={"sp": sp + 1 if up else sp - 1},
            device_id_type=MESH,
        )

    @pl.when(has_high)
    def _():
        halo_copy(True).start()

    @pl.when(has_low)
    def _():
        halo_copy(False).start()

    def to_parts(src, dst, ssem, rsem):
        for d in range(1, NX):
            part = lax.rem(x + d, NX)
            send(src.at[part], dst.at[x], ssem.at[d - 1], rsem.at[d - 1], {"fs": part})

    def from_parts(dst, ssem, rsem):
        for d in range(1, NX):
            arrived(dst.at[lax.rem(x + NX - d, NX)], ssem.at[d - 1], rsem.at[d - 1], partner)

    to_parts(ql_send, ql_recv, ql_ssem, ql_rsem)
    ql_recv[x] = ql_send[x]

    @pl.when(jnp.logical_not(has_low))
    def _():
        gated[:, 0:HALO, :] = edge

    @pl.when(jnp.logical_not(has_high))
    def _():
        gated[:, HALO + count :, :] = edge

    g_keys.wait_ring(last)
    for half in (0, 1):
        for way in (0, 1):
            pair_keys(half, way, last)
    g_out.wait_first()
    g_out.start_ring(1)

    from_parts(ql_recv, ql_ssem, ql_rsem)
    latent_query = jnp.concatenate([ql_recv[k] for k in range(NX)], axis=1)
    latent_query = rms(latent_query, query_gain[...].astype(F32)).astype(BF16)
    query_all = dot(latent_query, query_up[...])
    cosine = wide[0, 0:count, 0:ROPE]
    sine = wide[1, 0:count, 0:ROPE]
    nothing = jnp.zeros((count, ROPE), F32)
    for h in range(heads):
        start = h * (NOPE + ROPE)
        plain = query_all[:, start : start + NOPE].astype(BF16)
        turned = query_all[:, start + NOPE : start + NOPE + ROPE]
        turned = turned * cosine + swap(turned) * sine
        absorbed = dot_t(plain, key_up[:, h * NOPE : (h + 1) * NOPE]).astype(BF16)
        rows = slice(h * count, (h + 1) * count)
        queries[0, rows, 0:KVR] = absorbed
        queries[1, rows, 0:KVR] = absorbed
        queries[0, rows, KVR:] = jnp.concatenate([turned, nothing], axis=1).astype(BF16)
        queries[1, rows, KVR:] = jnp.concatenate([nothing, turned], axis=1).astype(BF16)

    @pl.when(has_low)
    def _():
        halo_copy(True).wait_recv()

    @pl.when(has_high)
    def _():
        halo_copy(False).wait_recv()

    reach = conv_taps.shape[0] // 2
    columns = pl.ds(pl.multiple_of(x * GROUP, GROUP), GROUP)
    taps = conv_taps[:, columns].astype(F32)
    channel_gain = group_gain[x].astype(F32)
    for j in range(NX):
        wide[j, :, :] = gated[j].astype(F32)
        total = jnp.zeros((count, GROUP), F32)
        for t in range(2 * reach + 1):
            lo = HALO - reach + t
            total = total + wide[j, lo : lo + count, :] * taps[t : t + 1, :]
        centred = total - jnp.mean(total, axis=-1, keepdims=True)
        spread = jnp.mean(centred * centred, axis=-1, keepdims=True)
        conv_send[j] = jax.nn.silu(centred * lax.rsqrt(spread + EPS) * channel_gain).astype(BF16)
    to_parts(conv_send, conv_recv, cv_ssem, cv_rsem)
    conv_recv[x] = conv_send[x]

    other_keys = Gather(keys_all.at[other], nz, ny, z, y, keys_p_send, keys_p_recv, keys_r_send, keys_r_recv)
    for half in (0, 1):
        ref = other_keys.block(half, z if half == 0 else y)
        arrived(ref, pair0_send.at[half], pair0_recv.at[half], partner)
    for s in range(1, last + 1):
        for half in (0, 1):
            for way in (0, 1):
                ref = other_keys.ring_block(half, way, s, False)
                arrived(ref, pair_send.at[half, way, s - 1], pair_recv.at[half, way, s - 1], partner)

    scale = (NOPE + ROPE) ** (-0.5)
    factor = scale * math.log2(math.e)
    row_max[...] = jnp.full(row_max.shape, -1e30, F32)
    row_sum[...] = jnp.zeros(row_sum.shape, F32)
    acc[...] = jnp.zeros(acc.shape, F32)
    block_rows = ny * 2 * (quarter // 2)

    def attend(k, carry):
        pieces, values = [], []
        for core in (0, 1):
            block = keys_all[core, k].reshape(block_rows, 2 * KVR + 2 * ROPE)
            tail = block[:, 2 * KVR :]
            for low in (0, 1):
                value = block[:, low * KVR : (low + 1) * KVR]
                pieces.append(dot_t(queries[low], jnp.concatenate([value, tail], axis=1)))
                values.append(value)
        scores = jnp.concatenate(pieces, axis=1)
        before = row_max[...]
        now = jnp.maximum(before, jnp.max(scores, axis=1, keepdims=True))
        shrink = jnp.exp2((before - now) * factor)
        weights = jnp.exp2((scores - jnp.tile(now, (1, scores.shape[1] // 128))) * factor)
        row_sum[...] = row_sum[...] * shrink + jnp.sum(weights, axis=1, keepdims=True)
        row_max[...] = now
        added = dot(weights.astype(BF16), jnp.concatenate(values, axis=0))
        acc[...] = acc[...] * jnp.tile(shrink, (1, KVR // 128)) + added
        return carry

    groups = nz // last
    for s in range(1, last + 1):
        lax.fori_loop((s - 1) * groups, s * groups, attend, 0)
        g_out.wait_ring(s)
        if s < last:
            g_out.start_ring(s + 1)

    for h in range(heads):
        rows = slice(h * count, (h + 1) * count)
        attended = (acc[rows, :] / jnp.tile(row_sum[rows, :], (1, KVR // 128))).astype(BF16)
        head_out[:, h * VDIM : (h + 1) * VDIM] = dot(attended, value_up[:, h * VDIM : (h + 1) * VDIM]).astype(BF16)
        logs = row_max[rows, :] * scale + jnp.log(row_sum[rows, :])
        log_weight[h : h + 1, :] = jnp.transpose(logs)[0:1, :]

    from_parts(conv_recv, cv_ssem, cv_rsem)
    mixed = jnp.concatenate([head_out[...]] + [conv_recv[k] for k in range(NX)], axis=1)
    zs = nz // 2
    width = zs * ny * 2 * out_all.shape[3]

    def columns_of(core):
        return dot_t(mixed, out_all[pl.ds(core * zs, zs)].reshape(width, mixed.shape[1]))

    part_send[...] = columns_of(other).astype(BF16)
    send(part_send, part_recv, fin_sem.at[0], fin_sem.at[1], partner)
    kept = columns_of(c).astype(BF16).astype(F32)
    arrived(part_recv, fin_sem.at[0], fin_sem.at[1], partner)
    out[...] = (kept + part_recv[...].astype(F32)).astype(BF16)

    for copy in sent:
        copy.wait_send()
    for gather in (g_down, g_keys, g_out):
        gather.finish()

    @pl.when(has_high)
    def _():
        halo_copy(True).wait_send()

    @pl.when(has_low)
    def _():
        halo_copy(False).wait_send()


def per_device(
    nz,
    ny,
    tokens,
    norm_gain,
    query_down,
    query_gain,
    latent_down,
    latent_gain,
    rope_down,
    query_up,
    key_up,
    value_up,
    glu_value,
    glu_gate,
    conv_taps,
    group_gain,
    head_proj,
    channel_proj,
):
    count, depth = tokens.shape
    shard = query_down.shape[0]
    x = lax.axis_index("fs")
    heads = key_up.shape[1] // NOPE

    def plane(a):
        return lax.dynamic_slice_in_dim(a, x * GROUP, GROUP, 1)

    down_shard = jnp.concatenate([plane(glu_value), plane(glu_gate), plane(query_down)], axis=1)
    down_shard = down_shard.reshape(2, shard // 2, 3 * GROUP)
    out_cols = head_proj.shape[1]
    mixed = head_proj.shape[0] + channel_proj.shape[0]
    out_shard = jnp.concatenate([head_proj, channel_proj], axis=0).T.reshape(2, out_cols // 2, mixed)
    freq = (BASE ** (-np.arange(ROPE // 4, dtype=np.float64) / (ROPE // 4))).astype(np.float32)
    inv_freq = jnp.asarray(np.tile(freq, 4)[None, :])
    key_rows = count // 8
    key_width = 2 * KVR + 2 * ROPE
    hops = max(nz, ny) - 1
    last = max(nz, ny) // 2
    dma = pltpu.SemaphoreType.DMA
    gather_sems = [dma((2, hops)), dma((2, hops)), dma((2, 2, last)), dma((2, 2, last))]
    vmem = pl.BlockSpec(memory_space=pltpu.VMEM)
    hbm = pl.BlockSpec(memory_space=pltpu.HBM)
    operands = (
        (tokens, vmem),
        (norm_gain[None, :], vmem),
        (down_shard, hbm),
        (query_gain[None, :], vmem),
        (latent_down, vmem),
        (latent_gain[None, :], vmem),
        (rope_down, vmem),
        (query_up, vmem),
        (key_up, vmem),
        (value_up, vmem),
        (conv_taps, vmem),
        (group_gain.reshape(NX, 1, GROUP), vmem),
        (out_shard, hbm),
        (inv_freq, vmem),
    )
    half_cols = nz * ny * out_cols // 2
    return pl.pallas_call(
        functools.partial(kernel, nz, ny),
        out_shape=(
            jax.ShapeDtypeStruct((count, half_cols), BF16),
            jax.ShapeDtypeStruct((heads, count), F32),
        ),
        in_specs=[spec for _, spec in operands],
        out_specs=(vmem, vmem),
        scratch_shapes=[
            pltpu.VMEM((NX, 2, count // 2, depth), BF16),
            pltpu.VMEM((nz, ny, 2, shard // 2, 3 * GROUP), BF16),
            pltpu.VMEM((2, nz, ny, 2, key_rows, key_width), BF16),
            pltpu.VMEM((nz, ny, 2, out_cols // 2, mixed), BF16),
            pltpu.VMEM((NX, count, GROUP), F32),
            pltpu.VMEM((NX, count, GROUP), F32),
            pltpu.VMEM((NX, count + 2 * HALO, GROUP), BF16),
            pltpu.VMEM((NX, count + 2 * HALO, GROUP), F32),
            pltpu.VMEM((NX, count, GROUP), BF16),
            pltpu.VMEM((NX, count, GROUP), BF16),
            pltpu.VMEM((2, heads * count, KVR + 2 * ROPE), BF16),
            pltpu.VMEM((heads * count, 128), F32),
            pltpu.VMEM((heads * count, 128), F32),
            pltpu.VMEM((heads * count, KVR), F32),
            pltpu.VMEM((count, heads * VDIM), BF16),
            pltpu.VMEM((count, half_cols), BF16),
            pltpu.VMEM((count, half_cols), BF16),
            dma((2,)),
            *gather_sems,
            *gather_sems,
            *gather_sems,
            dma((2, 2, last)),
            dma((2, 2, last)),
            dma((2,)),
            dma((2,)),
            dma((3,)),
            dma((3,)),
            dma((3,)),
            dma((3,)),
            dma((3,)),
            dma((3,)),
            dma((3,)),
            dma((3,)),
            dma((2,)),
            dma((2,)),
            dma((2,)),
        ],
        compiler_params=pltpu.CompilerParams(
            collective_id=0, has_side_effects=True, vmem_limit_bytes=60 * 1024 * 1024
        ),
    )(*[value for value, _ in operands])


def solution(mesh):
    sp = mesh.shape["sp"]
    ny = math.isqrt(sp)
    nz = sp // ny
    in_specs = (
        P(("fs", "sp"), None),
        P(),
        P("sp", None),
        P(),
        P(),
        P(),
        P(),
        P(None, "tp"),
        P(None, "tp"),
        P(None, "tp"),
        P("sp", "tp"),
        P("sp", "tp"),
        P(None, "tp"),
        P("tp"),
        P("tp", "sp"),
        P("tp", "sp"),
    )
    out_specs = (P(("fs", "sp"), "tp"), P("tp", ("fs", "sp")))
    return jax.shard_map(
        functools.partial(per_device, nz, ny), mesh=mesh, in_specs=in_specs, out_specs=out_specs, check_vma=False
    )
```

time: 296 us -> 98.9 us (0.33)
  waiting for transfers between devices: 211 us -> 0 us
  Pallas kernels: 0 us -> 86.8 us
  matrix products: 33.1 us -> 0 us
  other arithmetic: 23.5 us -> 2.03 us
  between operations: 14 us -> 0.67 us
  blocking collectives: 8.59 us -> 0 us
  local copies, waits for them, and re-layouts: 2.22 us -> 9.07 us
  starting transfers between devices: 3.33 us -> 0 us
    all_gather x3 -> x0, waiting for transfers between devices: 211 us -> none  [the longest x1 84.6 us: in_one_piece(): result = lax.all_gather(both, axis, axis=dim, tiled=True)]
    pallas_call x0 -> x1, Pallas kernels: none -> 86.8 us  [per_device(): pl.pallas_call(functools.partial(kernel, nz, ny), out_shape=(jax.ShapeDty...]
    dot_general x10 -> x0, matrix products: 33.1 us -> none  [the longest x1 10.9 us: per_device(): jnp.einsum('hqc,kc->hqk', queries, block_keys, preferred_element_type=jnp...]
    reduce_sum x5 -> x0, other arithmetic: 11.3 us -> none  [the longest x1 8.7 us: per_device(): new_sum = jnp.sum(weights, axis=2)]
    all_to_all x1 -> x0, blocking collectives: 8.59 us -> none  [sent_and_summed(): lax.all_to_all(tiles, axis, split_axis=0, concat_axis=0, tiled=True)]
    convert_element_type x11 -> x0, other arithmetic: 4.24 us -> none  [the longest x3 2.03 us: rms_scale(): return values * inv_rms * scale_gain.astype(jnp.float32)]
    broadcast_in_dim x0 -> x3, local copies, waits for them, and re-layouts: none -> 3.81 us  [the longest x1 1.28 us: per_device(): norm_gain[None, :]]
    ppermute x2 -> x0, starting transfers between devices: 3.21 us -> none  [the longest x1 1.92 us: padded_2(): lax.ppermute(lax.slice_in_dim(block, block.shape[dim] - width, None, axis...]
  transfers between devices with their start and end apart: 5 -> 0, of which waited for: 3 -> 0; matrix products, arithmetic and copies ran while one was open for 18% -> 0% of each run, Pallas kernels for 0% -> 0%
where the time goes in v1:
time: 98.9 us; the launch traced here: 98.6 us
  Pallas kernels  86.8 us (88%)
  local copies, waits for them, and re-layouts  9.07 us (9%)
  other arithmetic  2.03 us (2%)
    pallas_call x1, Pallas kernels, per_device(): pl.pallas_call(functools.partial(kernel, nz, ny), out_shape=(jax.ShapeDty...  86.8 us
    unnamed x9, local copies, waits for them, and re-layouts  3.27 us

profile of v1, /device:TPU:1, one launch (start us, length us, event | category | flops | bytes accessed | tf_op | source)
XLA Modules:
  0.0 98.6 jit_solution(11103026160242327859)
XLA Ops:
  0.6 0.0 copy-start
  0.6 0.0 copy-start.1
  0.7 1.3 %broadcast_in_dim.11.latent_gain = bf16[1,256]{1,0:T(2,128)(2,1)} reshape(bf16[256]{0:T(256)(128)(2,1)} %param.22) | data formatting | bytes 1024 | tf_op jit(solution)/shard_map/broadcast_in_dim | solution.py:577
  1.9 1.3 %broadcast_in_dim.10.query_gain = bf16[1,512]{1,0:T(2,128)(2,1)} reshape(bf16[512]{0:T(512)(128)(2,1)} %param.20) | data formatting | bytes 2048 | tf_op jit(solution)/shard_map/broadcast_in_dim | solution.py:575
  3.2 1.3 %copy.21.group_gain = bf16[4,1,128]{2,1,0:T(2,128)(2,1)} copy(bf16[4,1,128]{2,0,1:T(4,128)(2,1)} %bitcast.7) | data formatting | bytes 2048 | tf_op jit(solution)/shard_map/reshape | solution.py:583
  4.5 1.3 %broadcast_in_dim.9.norm_gain = bf16[1,2048]{1,0:T(2,128)(2,1)} reshape(bf16[2048]{0:T(1024)(128)(2,1)} %param.18) | data formatting | bytes 8192 | tf_op jit(solution)/shard_map/broadcast_in_dim | solution.py:573
  5.7 0.0 copy-done
  5.7 0.7 constant_dynamic-slice_fusion
  6.5 0.6 pad_maximum_fusion.1
  7.1 1.4 %pad_maximum_fusion = bf16[1024,32]{0,1:T(8,128)(2,1)} fusion(bf16[512,32]{0,1:T(8,128)(2,1)} %param.32, bf16[512,32]{0,1:T(8,128)(2,1)} %param.31), kind=kLoop, calls=%fused_computation | loop fusion | flops 131072 | bytes 131072 | tf_op jit(solution)/shard_map/concatenate | solution.py:560
  8.5 0.0 copy-done.1
  8.5 1.0 %copy.20.rope_down = bf16[2048,64]{1,0:T(8,128)(2,1)} copy(bf16[2048,64]{0,1:T(8,128)(2,1)S(1)} %copy-done.1) | data formatting | bytes 524288 | tf_op args[6]
  9.5 86.8 %shard_map.176 = (bf16[128,1024]{1,0:T(8,128)(2,1)}, f32[4,128]{1,0:T(4,128)}) custom-call(bf16[128,2048]{1,0:T(8,128)(2,1)} %tokens.1, bf16[1,2048]{1,0:T(2,128)(2,1)} %broadcast_in_dim.9.norm_gain, bf16[2,16,384]{2,1,0:T(8,128)(2,1)} %bitcast.6, bf16[1,512]{1,0:T(2,128)(2,1)} %broadcast_in_dim.10.query_gain, bf16[2048,256]{1,0:T(8,128)(2,1)} %latent_down.1, ...), custom_call_target="tpu_custom_call" | custom-call | tf_op jit(solution)/shard_map/pallas_call | solution.py:588
  96.3 0.0 copy-start.2
  96.3 1.7 %copy.24 = bf16[128,1024]{1,0:T(8,128)(2,1)} copy(bf16[128,1024]{1,0:T(8,128)(2,1)} %get-tuple-element.6) | data formatting | bytes 524288
  98.0 0.0 copy-done.2
  98.0 0.6 copy.25
  (1 shorter events, 0.0 us)
Async XLA Ops:
  0.6 5.1 %copy-start = (bf16[32,512]{1,0:T(8,128)(2,1)S(1)}, bf16[32,512]{1,0:T(8,128)(2,1)}, u32[]{:S(2)}) copy-start(bf16[32,512]{1,0:T(8,128)(2,1)} %param.27) | copy-start | bytes 98308
  0.6 7.8 %copy-start.1 = (bf16[2048,64]{0,1:T(8,128)(2,1)S(1)}, bf16[2048,64]{0,1:T(8,128)(2,1)}, u32[]{:S(2)}) copy-start(bf16[2048,64]{0,1:T(8,128)(2,1)} %param.23) | copy-start | bytes 786436
  96.3 1.7 %copy-start.2 = (f32[4,128]{1,0:T(4,128)S(1)}, f32[4,128]{1,0:T(4,128)}, u32[]{:S(2)}) copy-start(f32[4,128]{1,0:T(4,128)} %get-tuple-element.7) | copy-start | bytes 6148

commit v2 on v1

v2 whole, which is shorter than its diff:
```python
import functools
import math

import jax
import jax.numpy as jnp
import numpy as np
from jax import lax
from jax.experimental import pallas as pl
from jax.experimental.pallas import tpu as pltpu
from jax.sharding import PartitionSpec as P

NOPE = 128
ROPE = 64
VDIM = 128
KVR = 256
GROUP = 128
GRID_W = 64
EPS = 1e-06
BASE = 10000.0
HALO = 16
NX = 4
F32 = jnp.float32
BF16 = jnp.bfloat16
MESH = pl.DeviceIdType.MESH


def dot(a, b):
    return jnp.dot(a, b, preferred_element_type=F32)


def dot_t(a, b):
    return lax.dot_general(a, b, (((1,), (1,)), ((), ())), preferred_element_type=F32)


def rms(values, gain):
    inv = lax.rsqrt(jnp.mean(values * values, axis=-1, keepdims=True) + EPS)
    return values * inv * gain


def swap(v):
    half = v.shape[-1] // 2
    return jnp.concatenate([v[:, half:], v[:, :half]], axis=-1)


class Gather:
    def __init__(self, view, nz, ny, z, y, p_send, p_recv, r_send, r_recv):
        self.view, self.size, self.pos = view, (nz, ny), (z, y)
        self.p_send, self.p_recv, self.r_send, self.r_recv = p_send, p_recv, r_send, r_recv
        self.sent = []

    def device(self, axis, k):
        z, y = (k, self.pos[1]) if axis == 0 else (self.pos[0], k)
        return {"sp": z * self.size[1] + y}

    def first_copy(self, half, d, outgoing):
        axis = 1 - half
        n = self.size[axis]
        me = self.pos[axis]
        source = me if outgoing else lax.rem(me + n - d, n)
        z, y = (source, self.pos[1]) if axis == 0 else (self.pos[0], source)
        ref = self.view.at[z, y, half]
        return pltpu.make_async_remote_copy(
            src_ref=ref,
            dst_ref=ref,
            send_sem=self.p_send.at[half, d - 1],
            recv_sem=self.p_recv.at[half, d - 1],
            device_id=self.device(axis, lax.rem(me + d, n)),
            device_id_type=MESH,
        )

    def start_first(self):
        for half in (0, 1):
            for d in range(1, self.size[1 - half]):
                copy = self.first_copy(half, d, True)
                copy.start()
                self.sent.append(copy)

    def wait_first(self):
        for half in (0, 1):
            for d in range(1, self.size[1 - half]):
                self.first_copy(half, d, False).wait_recv()

    def block(self, half, k, part=None):
        n = self.size[1 - half]
        rows = slice(None) if part is None else pl.ds(part * (n // 2), n // 2)
        return self.view.at[k, rows, 0] if half == 0 else self.view.at[rows, k, 1]

    def steps(self, half):
        return self.size[half] // 2

    def ring_block(self, half, way, s, outgoing):
        n = self.size[half]
        back = s - 1 if outgoing else s
        sign = 1 - 2 * way
        k = lax.rem(self.pos[half] - sign * back + n, n)
        return self.block(half, k, way if s == n // 2 else None)

    def ring_copy(self, half, way, s, outgoing):
        n = self.size[half]
        ref = self.ring_block(half, way, s, outgoing)
        target = lax.rem(self.pos[half] + (1 - 2 * way) + n, n)
        return pltpu.make_async_remote_copy(
            src_ref=ref,
            dst_ref=ref,
            send_sem=self.r_send.at[half, way, s - 1],
            recv_sem=self.r_recv.at[half, way, s - 1],
            device_id=self.device(half, target),
            device_id_type=MESH,
        )

    def start_ring(self, s):
        for half in (0, 1):
            for way in (0, 1):
                copy = self.ring_copy(half, way, s, True)
                copy.start()
                self.sent.append(copy)

    def wait_ring(self, s):
        for half in (0, 1):
            for way in (0, 1):
                self.ring_copy(half, way, s, False).wait_recv()

    def direct_copy(self, half, d, outgoing):
        n = self.size[half]
        me = self.pos[half]
        ref = self.block(half, me if outgoing else lax.rem(me + n - d, n))
        return pltpu.make_async_remote_copy(
            src_ref=ref,
            dst_ref=ref,
            send_sem=self.r_send.at[half, d - 1],
            recv_sem=self.r_recv.at[half, d - 1],
            device_id=self.device(half, lax.rem(me + d, n)),
            device_id_type=MESH,
        )

    def start_direct(self):
        for half in (0, 1):
            for d in range(1, self.size[half]):
                copy = self.direct_copy(half, d, True)
                copy.start()
                self.sent.append(copy)

    def wait_direct(self):
        for half in (0, 1):
            for d in range(1, self.size[half]):
                self.direct_copy(half, d, False).wait_recv()

    def pass_on(self, s, each=None):
        for half in (0, 1):
            for way in (0, 1):
                self.ring_copy(half, way, s, False).wait_recv()
                if s < self.steps(half):
                    copy = self.ring_copy(half, way, s + 1, True)
                    copy.start()
                    self.sent.append(copy)
                if each is not None:
                    each(half, way, s)

    def finish(self):
        for copy in self.sent:
            copy.wait_send()


IN_HBM = (
    "tokens",
    "latent_down",
    "rope_down",
    "query_up",
    "key_up",
    "value_up",
    "conv_taps",
)
SHARDS = ("query_down", "glu_value", "glu_gate", "head_proj", "channel_proj")
GAINS = ("norm_gain", "query_gain", "latent_gain", "group_gain", "inv_freq")
SCRATCH = (
    "normed4",
    "query_w",
    "glu_w",
    "keys_all",
    "out_all",
    "ql_send",
    "ql_recv",
    "gated",
    "wide",
    "conv_send",
    "conv_recv",
    "queries",
    "row_max",
    "row_sum",
    "acc",
    "head_out",
    "part_send",
)
SEMS = (
    "load_sem",
    "shard_sem",
    "qw_ps",
    "qw_pr",
    "qw_rs",
    "qw_rr",
    "glu_ps",
    "glu_pr",
    "glu_rs",
    "glu_rr",
    "keys_ps",
    "keys_pr",
    "keys_rs",
    "keys_rr",
    "out_ps",
    "out_pr",
    "out_rs",
    "out_rr",
    "pair_send",
    "pair_recv",
    "pair0_send",
    "pair0_recv",
    "x_send",
    "x_recv",
    "xp_send",
    "xp_recv",
    "ql_ssem",
    "ql_rsem",
    "cv_ssem",
    "cv_rsem",
    "halo_ssem",
    "halo_rsem",
    "fin_sem",
)
OUTS = ("kept", "part_recv", "log_weight")


def kernel(nz, ny, *refs):
    names = IN_HBM + SHARDS + GAINS + OUTS + SCRATCH + tuple("v_" + n for n in IN_HBM) + SEMS
    r = dict(zip(names, refs, strict=True))
    body(nz, ny, r)


def body(nz, ny, r):
    sp = lax.axis_index("sp")
    x = lax.axis_index("fs")
    c = lax.axis_index("tp")
    z, y = sp // ny, lax.rem(sp, ny)
    other = 1 - c
    tokens, latent_down, rope_down = r["v_tokens"], r["v_latent_down"], r["v_rope_down"]
    query_up, key_up, value_up, conv_taps = (r["v_" + n] for n in ("query_up", "key_up", "value_up", "conv_taps"))
    normed4, keys_all, out_all, gated, wide = (r[n] for n in ("normed4", "keys_all", "out_all", "gated", "wide"))
    query_w, glu_w, queries = r["query_w"], r["glu_w"], r["queries"]
    row_max, row_sum, acc = r["row_max"], r["row_sum"], r["acc"]
    count, depth = tokens.shape
    half_rows = count // 2
    heads = key_up.shape[1] // NOPE
    partner = {"tp": other}

    barrier = pltpu.get_barrier_semaphore()

    def greet(**where):
        pl.semaphore_signal(barrier, inc=1, device_id=where, device_id_type=MESH)

    for d in range(1, ny):
        greet(sp=z * ny + lax.rem(y + d, ny))
    for d in range(1, nz):
        greet(sp=lax.rem(z + d, nz) * ny + y)
    for d in range(1, NX):
        greet(fs=lax.rem(x + d, NX))
    greet(tp=other)
    has_low = sp > 0
    has_high = sp < nz * ny - 1

    @pl.when(has_low)
    def _():
        greet(sp=sp - 1)

    @pl.when(has_high)
    def _():
        greet(sp=sp + 1)

    loads = {}
    for k, name in enumerate(IN_HBM):
        loads[name] = pltpu.make_async_copy(r[name], r["v_" + name], r["load_sem"].at[k])
        loads[name].start()
        if k == 0:
            columns = pl.ds(pl.multiple_of(x * GROUP, GROUP), GROUP)
            slot = (z, y)
            wide_out = r["head_proj"].shape[-1]
            shards = (
                (r["query_down"].at[:, :, columns], query_w.at[slot]),
                (r["glu_value"].at[:, :, columns], glu_w.at[z, y, :, :, pl.ds(0, GROUP)]),
                (r["glu_gate"].at[:, :, columns], glu_w.at[z, y, :, :, pl.ds(GROUP, GROUP)]),
                (r["head_proj"], out_all.at[z, y, :, :, pl.ds(0, wide_out)]),
                (r["channel_proj"], out_all.at[z, y, :, :, pl.ds(wide_out, wide_out)]),
            )
            shards = [pltpu.make_async_copy(a, b, r["shard_sem"].at[i]) for i, (a, b) in enumerate(shards)]
            for copy in shards:
                copy.start()

    g_query = Gather(query_w, nz, ny, z, y, r["qw_ps"], r["qw_pr"], r["qw_rs"], r["qw_rr"])
    g_glu = Gather(glu_w, nz, ny, z, y, r["glu_ps"], r["glu_pr"], r["glu_rs"], r["glu_rr"])
    keys_sems = (r["keys_ps"], r["keys_pr"], r["keys_rs"], r["keys_rr"])
    g_keys = Gather(keys_all.at[c], nz, ny, z, y, *keys_sems)
    other_keys = Gather(keys_all.at[other], nz, ny, z, y, *keys_sems)
    g_out = Gather(out_all, nz, ny, z, y, r["out_ps"], r["out_pr"], r["out_rs"], r["out_rr"])
    sent = []

    def send(src, dst, ssem, rsem, where):
        copy = pltpu.make_async_remote_copy(
            src_ref=src, dst_ref=dst, send_sem=ssem, recv_sem=rsem, device_id=where, device_id_type=MESH
        )
        copy.start()
        sent.append(copy)

    def arrived(dst, ssem, rsem):
        pltpu.make_async_remote_copy(
            src_ref=dst, dst_ref=dst, send_sem=ssem, recv_sem=rsem, device_id=partner, device_id_type=MESH
        ).wait_recv()

    at_row = lax.broadcasted_iota(jnp.int32, (count, ROPE), 0)
    lane = lax.broadcasted_iota(jnp.int32, (count, ROPE), 1)
    place = at_row + sp * count
    grid_row = (place // GRID_W).astype(F32)
    grid_col = lax.rem(place, GRID_W).astype(F32)
    angles = jnp.where(lax.rem(lane, ROPE // 2) < ROPE // 4, grid_row, grid_col) * r["inv_freq"][...]
    wide[0, 0:count, 0:ROPE] = jnp.cos(angles)
    wide[1, 0:count, 0:ROPE] = jnp.sin(angles) * jnp.where(lane < ROPE // 2, -1.0, 1.0)

    loads["tokens"].wait()
    gain = r["norm_gain"][...].astype(F32)[None, :]
    chunk = 32
    for k in range(count // chunk):
        rows = tokens[k * chunk : (k + 1) * chunk, :].astype(F32)
        value = rms(rows, gain).astype(BF16)
        which, first = divmod(k * chunk, half_rows)
        normed4[x, which, first : first + chunk, :] = value

    loads["latent_down"].wait()
    loads["rope_down"].wait()
    own = normed4[x, c]
    latent = rms(dot(own, latent_down[...]), r["latent_gain"][...].astype(F32)[None, :]).astype(BF16)
    rope_key = dot_t(own, rope_down[...])
    first = pl.multiple_of(c * half_rows, half_rows)
    rope_key = rope_key * wide[0, pl.ds(first, half_rows), 0:ROPE] + swap(rope_key) * wide[
        1, pl.ds(first, half_rows), 0:ROPE
    ]
    quarter = half_rows // 2
    rope_pair = jnp.concatenate([rope_key[:quarter], rope_key[quarter:]], axis=1).astype(BF16)
    for h in (0, 1):
        lo = h * (quarter // 2)
        hi = lo + quarter // 2
        keys_all[c, z, y, h, :, 0:KVR] = latent[lo:hi]
        keys_all[c, z, y, h, :, KVR : 2 * KVR] = latent[quarter + lo : quarter + hi]
        keys_all[c, z, y, h, :, 2 * KVR :] = rope_pair[lo:hi]

    for copy in shards:
        copy.wait()
    edges = has_low.astype(jnp.int32) + has_high.astype(jnp.int32)
    pl.semaphore_wait(barrier, (ny - 1) + (nz - 1) + (NX - 1) + 1 + edges)

    g_query.start_first()
    for way in (0, 1):
        mine = normed4.at[x, c]
        where = {"fs": lax.rem(x + (1 - 2 * way) + NX, NX)}
        send(mine, mine, r["x_send"].at[way], r["x_recv"].at[way], where)
    g_keys.start_first()
    g_glu.start_first()
    g_out.start_first()
    for name in IN_HBM[3:]:
        loads[name].wait()

    def pair_keys(half, way, s):
        block = g_keys.ring_block(half, way, s, False)
        sems = r["pair_send"].at[half, way, s - 1], r["pair_recv"].at[half, way, s - 1]
        send(block, block, *sems, partner)

    g_query.wait_first()
    g_query.start_direct()

    turn = 1 - 2 * c
    far = lax.rem(x + 2, NX)
    for way in (0, 1):
        src = lax.rem(x - (1 - 2 * way) + NX, NX)
        piece = normed4.at[src, c]
        arrived(piece, r["x_send"].at[way], r["x_recv"].at[way])
        send(piece, piece, r["xp_send"].at[way], r["xp_recv"].at[way], partner)
    onward = normed4.at[lax.rem(x - turn + NX, NX), c]
    send(onward, onward, r["x_send"].at[2], r["x_recv"].at[2], {"fs": lax.rem(x + turn + NX, NX)})

    last = nz // 2
    g_keys.wait_first()
    g_keys.start_ring(1)
    own_block = (g_keys.block(0, z), g_keys.block(1, y))
    for half in (0, 1):
        send(own_block[half], own_block[half], r["pair0_send"].at[half], r["pair0_recv"].at[half], partner)
    g_glu.wait_first()
    g_glu.start_ring(1)
    g_out.wait_first()
    g_out.start_ring(1)

    g_keys.pass_on(1, pair_keys)
    g_glu.pass_on(1)
    piece = normed4.at[far, c]
    arrived(piece, r["x_send"].at[2], r["x_recv"].at[2])
    send(piece, piece, r["xp_send"].at[2], r["xp_recv"].at[2], partner)
    g_out.pass_on(1)

    def to_parts(src, dst, ssem, rsem):
        for d in range(1, NX):
            part = lax.rem(x + d, NX)
            send(src.at[part], dst.at[x], ssem.at[d - 1], rsem.at[d - 1], {"fs": part})

    def from_parts(dst, ssem, rsem):
        for d in range(1, NX):
            arrived(dst.at[lax.rem(x + NX - d, NX)], ssem.at[d - 1], rsem.at[d - 1])

    g_query.wait_direct()
    for k in range(3):
        src = far if k == 2 else lax.rem(x - (1 - 2 * k) + NX, NX)
        arrived(normed4.at[src, other], r["xp_send"].at[k], r["xp_recv"].at[k])
    ql_send, ql_recv = r["ql_send"], r["ql_recv"]
    everyone = normed4[...].reshape(NX * count, depth)
    ql_send[...] = dot(everyone, query_w[...].reshape(depth, GROUP)).reshape(NX, count, GROUP)
    to_parts(ql_send, ql_recv, r["ql_ssem"], r["ql_rsem"])
    ql_recv[x] = ql_send[x]

    g_keys.pass_on(2, pair_keys)
    g_glu.pass_on(2)
    g_out.pass_on(2)

    from_parts(ql_recv, r["ql_ssem"], r["ql_rsem"])
    latent_query = jnp.concatenate([ql_recv[k] for k in range(NX)], axis=1)
    latent_query = rms(latent_query, r["query_gain"][...].astype(F32)[None, :]).astype(BF16)
    query_all = dot(latent_query, query_up[...])
    cosine = wide[0, 0:count, 0:ROPE]
    sine = wide[1, 0:count, 0:ROPE]
    nothing = jnp.zeros((count, ROPE), F32)
    for h in range(heads):
        start = h * (NOPE + ROPE)
        plain = query_all[:, start : start + NOPE].astype(BF16)
        turned = query_all[:, start + NOPE : start + NOPE + ROPE]
        turned = turned * cosine + swap(turned) * sine
        absorbed = dot_t(plain, key_up[:, h * NOPE : (h + 1) * NOPE]).astype(BF16)
        rows = slice(h * count, (h + 1) * count)
        queries[0, rows, 0:KVR] = absorbed
        queries[1, rows, 0:KVR] = absorbed
        queries[0, rows, KVR:] = jnp.concatenate([turned, nothing], axis=1).astype(BF16)
        queries[1, rows, KVR:] = jnp.concatenate([nothing, turned], axis=1).astype(BF16)

    scale = (NOPE + ROPE) ** (-0.5)
    factor = scale * math.log2(math.e)
    row_max[...] = jnp.full(row_max.shape, -1e30, F32)
    row_sum[...] = jnp.zeros(row_sum.shape, F32)
    acc[...] = jnp.zeros(acc.shape, F32)
    lines = quarter // 2

    def attend(k, carry):
        odd = lax.rem(k, 2)
        step = odd * (lax.div(k, 2) + 1) - (1 - odd) * lax.div(k, 2)
        row = lax.rem(z + step + nz, nz)
        column = lax.rem(y + step + ny, ny)
        pieces, values = [], []
        for core in (0, 1):
            upper = keys_all[core, row, :, 0].reshape(ny * lines, 2 * KVR + 2 * ROPE)
            lower = keys_all[core, :, column, 1].reshape(nz * lines, 2 * KVR + 2 * ROPE)
            block = jnp.concatenate([upper, lower], axis=0)
            tail = block[:, 2 * KVR :]
            for low in (0, 1):
                value = block[:, low * KVR : (low + 1) * KVR]
                pieces.append(dot_t(queries[low], jnp.concatenate([value, tail], axis=1)))
                values.append(value)
        scores = jnp.concatenate(pieces, axis=1)
        before = row_max[...]
        now = jnp.maximum(before, jnp.max(scores, axis=1, keepdims=True))
        shrink = jnp.exp2((before - now) * factor)
        weights = jnp.exp2((scores - jnp.tile(now, (1, scores.shape[1] // 128))) * factor)
        row_sum[...] = row_sum[...] * shrink + jnp.sum(weights, axis=1, keepdims=True)
        row_max[...] = now
        added = dot(weights.astype(BF16), jnp.concatenate(values, axis=0))
        acc[...] = acc[...] * jnp.tile(shrink, (1, KVR // 128)) + added
        return carry

    def pair_arrived(s):
        for half in (0, 1):
            for way in (0, 1):
                ref = other_keys.ring_block(half, way, s, False)
                arrived(ref, r["pair_send"].at[half, way, s - 1], r["pair_recv"].at[half, way, s - 1])

    g_keys.pass_on(3, pair_keys)
    g_glu.pass_on(3)
    for half in (0, 1):
        ref = other_keys.block(half, z if half == 0 else y)
        arrived(ref, r["pair0_send"].at[half], r["pair0_recv"].at[half])
    pair_arrived(1)
    lax.fori_loop(0, 3, attend, 0)
    g_out.pass_on(3)
    pair_arrived(2)
    lax.fori_loop(3, 5, attend, 0)
    g_keys.pass_on(4, pair_keys)
    pair_arrived(3)
    lax.fori_loop(5, 7, attend, 0)

    g_glu.pass_on(4)
    glu_weights = glu_w[...].reshape(depth, 2 * GROUP)
    for j in range(NX):
        product = dot(normed4[j].reshape(count, depth), glu_weights)
        gated[j, HALO : HALO + count, :] = (product[:, :GROUP] * jax.nn.sigmoid(product[:, GROUP:])).astype(BF16)

    low_src, high_src = gated.at[:, pl.ds(HALO, HALO)], gated.at[:, pl.ds(count, HALO)]
    low_dst, high_dst = gated.at[:, pl.ds(0, HALO)], gated.at[:, pl.ds(HALO + count, HALO)]

    def halo_copy(up):
        src, dst = (high_src, low_dst) if up else (low_src, high_dst)
        k = 0 if up else 1
        return pltpu.make_async_remote_copy(
            src_ref=src,
            dst_ref=dst,
            send_sem=r["halo_ssem"].at[k],
            recv_sem=r["halo_rsem"].at[k],
            device_id={"sp": sp + 1 if up else sp - 1},
            device_id_type=MESH,
        )

    @pl.when(has_high)
    def _():
        halo_copy(True).start()

    @pl.when(has_low)
    def _():
        halo_copy(False).start()

    edge = jnp.zeros((NX, HALO, GROUP), BF16)

    @pl.when(jnp.logical_not(has_low))
    def _():
        gated[:, 0:HALO, :] = edge

    @pl.when(jnp.logical_not(has_high))
    def _():
        gated[:, HALO + count :, :] = edge

    pair_arrived(4)
    lax.fori_loop(7, 8, attend, 0)

    @pl.when(has_low)
    def _():
        halo_copy(True).wait_recv()

    @pl.when(has_high)
    def _():
        halo_copy(False).wait_recv()

    conv_send, conv_recv = r["conv_send"], r["conv_recv"]
    reach = conv_taps.shape[0] // 2
    taps = conv_taps[:, columns].astype(F32)
    gains = r["group_gain"][...].astype(F32)[None, :]
    channel_gain = gains[:, :GROUP]
    for k in range(1, NX):
        channel_gain = jnp.where(x == k, gains[:, k * GROUP : (k + 1) * GROUP], channel_gain)
    for j in range(NX):
        wide[j, :, :] = gated[j].astype(F32)
        total = jnp.zeros((count, GROUP), F32)
        for t in range(2 * reach + 1):
            lo = HALO - reach + t
            total = total + wide[j, lo : lo + count, :] * taps[t : t + 1, :]
        centred = total - jnp.mean(total, axis=-1, keepdims=True)
        spread = jnp.mean(centred * centred, axis=-1, keepdims=True)
        conv_send[j] = jax.nn.silu(centred * lax.rsqrt(spread + EPS) * channel_gain).astype(BF16)
    to_parts(conv_send, conv_recv, r["cv_ssem"], r["cv_rsem"])
    conv_recv[x] = conv_send[x]

    head_out, log_weight = r["head_out"], r["log_weight"]
    for h in range(heads):
        rows = slice(h * count, (h + 1) * count)
        attended = (acc[rows, :] / jnp.tile(row_sum[rows, :], (1, KVR // 128))).astype(BF16)
        head_out[:, h * VDIM : (h + 1) * VDIM] = dot(attended, value_up[:, h * VDIM : (h + 1) * VDIM]).astype(BF16)
        logs = row_max[rows, :] * scale + jnp.log(row_sum[rows, :])
        log_weight[h : h + 1, :] = jnp.transpose(logs)[0:1, :]

    from_parts(conv_recv, r["cv_ssem"], r["cv_rsem"])
    mixed = jnp.concatenate([head_out[...]] + [conv_recv[k] for k in range(NX)], axis=1)
    zs = nz // 2
    width = zs * ny * 2 * out_all.shape[3]
    part_send, part_recv = r["part_send"], r["part_recv"]
    g_out.pass_on(4)

    def columns_of(core):
        return dot_t(mixed, out_all[pl.ds(core * zs, zs)].reshape(width, mixed.shape[1])).astype(BF16)

    part_send[...] = columns_of(other)
    send(part_send, part_recv, r["fin_sem"].at[0], r["fin_sem"].at[1], partner)
    r["kept"][...] = columns_of(c)
    arrived(part_recv, r["fin_sem"].at[0], r["fin_sem"].at[1])

    for copy in sent:
        copy.wait_send()
    for gather in (g_query, g_glu, g_keys, g_out):
        gather.finish()

    @pl.when(has_high)
    def _():
        halo_copy(True).wait_send()

    @pl.when(has_low)
    def _():
        halo_copy(False).wait_send()


def per_device(
    nz,
    ny,
    tokens,
    norm_gain,
    query_down,
    query_gain,
    latent_down,
    latent_gain,
    rope_down,
    query_up,
    key_up,
    value_up,
    glu_value,
    glu_gate,
    conv_taps,
    group_gain,
    head_proj,
    channel_proj,
):
    count, depth = tokens.shape
    heads = key_up.shape[1] // NOPE

    def halves(a):
        return a.reshape(2, a.shape[0] // 2, a.shape[1])

    freq = (BASE ** (-np.arange(ROPE // 4, dtype=np.float64) / (ROPE // 4))).astype(np.float32)
    given = {
        "tokens": tokens,
        "latent_down": latent_down,
        "rope_down": rope_down.T,
        "query_up": query_up,
        "key_up": key_up,
        "value_up": value_up,
        "conv_taps": conv_taps,
        "query_down": halves(query_down),
        "glu_value": halves(glu_value),
        "glu_gate": halves(glu_gate),
        "head_proj": halves(head_proj.T),
        "channel_proj": halves(channel_proj.T),
        "norm_gain": norm_gain,
        "query_gain": query_gain,
        "latent_gain": latent_gain,
        "group_gain": group_gain,
        "inv_freq": jnp.asarray(np.tile(freq, 4)[None, :]),
    }
    shard = query_down.shape[0] // 2
    out_cols = head_proj.shape[1]
    mixed = head_proj.shape[0] + channel_proj.shape[0]
    half_cols = nz * ny * out_cols // 2
    hops = max(nz, ny) - 1
    last = max(nz, ny) // 2
    dma = pltpu.SemaphoreType.DMA
    vmem = pl.BlockSpec(memory_space=pltpu.VMEM)
    hbm = pl.BlockSpec(memory_space=pltpu.HBM)

    def buf(*shape, dtype=BF16):
        return pltpu.VMEM(shape, dtype)

    ring = [dma((2, hops)), dma((2, hops)), dma((2, 2, last)), dma((2, 2, last))]
    scratch = [
        buf(NX, 2, count // 2, depth),
        buf(nz, ny, 2, shard, GROUP),
        buf(nz, ny, 2, shard, 2 * GROUP),
        buf(2, nz, ny, 2, count // 8, 2 * KVR + 2 * ROPE),
        buf(nz, ny, 2, out_cols // 2, mixed),
        buf(NX, count, GROUP, dtype=F32),
        buf(NX, count, GROUP, dtype=F32),
        buf(NX, count + 2 * HALO, GROUP),
        buf(NX, count + 2 * HALO, GROUP, dtype=F32),
        buf(NX, count, GROUP),
        buf(NX, count, GROUP),
        buf(2, heads * count, KVR + 2 * ROPE),
        buf(heads * count, 128, dtype=F32),
        buf(heads * count, 128, dtype=F32),
        buf(heads * count, KVR, dtype=F32),
        buf(count, heads * VDIM),
        buf(count, half_cols),
        *[buf(*given[name].shape) for name in IN_HBM],
        dma((len(IN_HBM),)),
        dma((len(SHARDS),)),
        *[dma((2, hops))] * 4,
        *ring,
        *ring,
        *ring,
        dma((2, 2, last)),
        dma((2, 2, last)),
        dma((2,)),
        dma((2,)),
        *[dma((3,))] * 8,
        *[dma((2,))] * 3,
    ]
    kept, came, log_weight = pl.pallas_call(
        functools.partial(kernel, nz, ny),
        out_shape=(
            jax.ShapeDtypeStruct((count, half_cols), BF16),
            jax.ShapeDtypeStruct((count, half_cols), BF16),
            jax.ShapeDtypeStruct((heads, count), F32),
        ),
        in_specs=[hbm] * (len(IN_HBM) + len(SHARDS)) + [vmem] * len(GAINS),
        out_specs=(vmem, vmem, vmem),
        scratch_shapes=scratch,
        compiler_params=pltpu.CompilerParams(
            collective_id=0, has_side_effects=True, vmem_limit_bytes=60 * 1024 * 1024
        ),
    )(*[given[name] for name in IN_HBM + SHARDS + GAINS])
    return (kept.astype(F32) + came.astype(F32)).astype(BF16), log_weight


def solution(mesh):
    sp = mesh.shape["sp"]
    ny = math.isqrt(sp)
    nz = sp // ny
    in_specs = (
        P(("fs", "sp"), None),
        P(),
        P("sp", None),
        P(),
        P(),
        P(),
        P(),
        P(None, "tp"),
        P(None, "tp"),
        P(None, "tp"),
        P("sp", "tp"),
        P("sp", "tp"),
        P(None, "tp"),
        P("tp"),
        P("tp", "sp"),
        P("tp", "sp"),
    )
    out_specs = (P(("fs", "sp"), "tp"), P("tp", ("fs", "sp")))
    return jax.shard_map(
        functools.partial(per_device, nz, ny), mesh=mesh, in_specs=in_specs, out_specs=out_specs, check_vma=False
    )
```

time: 98.9 us -> 91.9 us (0.929)
  local copies, waits for them, and re-layouts: 9.07 us -> 0.58 us
  Pallas kernels: 86.8 us -> 88.7 us
    broadcast_in_dim x3 -> x0, local copies, waits for them, and re-layouts: 3.81 us -> none  [the longest x1 1.28 us: per_device(): norm_gain[None, :]]
    unnamed x9 -> x3, local copies, waits for them, and re-layouts: 3.27 us -> 0.58 us
    concatenate x2 -> x0, other arithmetic: 2.03 us -> none  [the longest x1 1.41 us: per_device(): jnp.concatenate([head_proj, channel_proj], axis=0)]
    pallas_call x1, Pallas kernels: 86.8 us -> 88.7 us  [per_device(): pl.pallas_call(functools.partial(kernel, nz, ny), out_shape=(jax.ShapeDty...]
    convert_element_type x0 -> x1, other arithmetic: none -> 1.8 us  [per_device(): return ((kept.astype(F32) + came.astype(F32)).astype(BF16), log_weight)]
    reshape x1 -> x0, local copies, waits for them, and re-layouts: 1.27 us -> none  [per_device(): group_gain.reshape(NX, 1, GROUP)]
where the time goes in v2:
time: 91.9 us; the launch traced here: 91.7 us
  Pallas kernels  88.7 us (97%)
  other arithmetic  1.8 us (2%)
    pallas_call x1, Pallas kernels, per_device(): pl.pallas_call(functools.partial(kernel, nz, ny), out_shape=(jax.ShapeDty...  88.7 us

profile of v2, /device:TPU:1, one launch (start us, length us, event | category | flops | bytes accessed | tf_op | source)
XLA Modules:
  0.0 91.7 jit_solution(14131349621139856958)
XLA Ops:
  0.6 88.7 %shard_map.176 = (bf16[128,1024]{1,0:T(8,128)(2,1)}, bf16[128,1024]{1,0:T(8,128)(2,1)}, f32[4,128]{1,0:T(4,128)}) custom-call(bf16[128,2048]{1,0:T(8,128)(2,1)} %refs_0_.1, bf16[2048,256]{1,0:T(8,128)(2,1)} %refs_1_.1, bf16[64,2048]{1,0:T(8,128)(2,1)} %bitcast.10, bf16[512,768]{1,0:T(8,128)(2,1)} %refs_3_.1, bf16[256,512]{1,0:T(8,128)(2,1)} %refs_4_.1, ...), custom_call_target="tpu_custom_call" | custom-call | tf_op jit(solution)/shard_map/pallas_call | solution.py:697
  89.3 0.0 copy-start
  89.3 1.8 %add_convert_fusion = bf16[128,1024]{1,0:T(8,128)(2,1)} fusion(bf16[128,1024]{1,0:T(8,128)(2,1)} %get-tuple-element.6, bf16[128,1024]{1,0:T(8,128)(2,1)} %get-tuple-element.5), kind=kLoop, calls=%fused_computation | loop fusion | flops 524288 | bytes 786432 | tf_op jit(solution)/shard_map/convert_element_type | solution.py:711
  91.1 0.0 copy-done
  91.1 0.6 copy.20
Async XLA Ops:
  89.3 1.8 %copy-start = (f32[4,128]{1,0:T(4,128)S(1)}, f32[4,128]{1,0:T(4,128)}, u32[]{:S(2)}) copy-start(f32[4,128]{1,0:T(4,128)} %get-tuple-element.11) | copy-start | bytes 6148

commit v3 on v2

--- a/solution.py
+++ b/solution.py
@@ -120,31 +120,6 @@
             for way in (0, 1):
                 self.ring_copy(half, way, s, False).wait_recv()
 
-    def direct_copy(self, half, d, outgoing):
-        n = self.size[half]
-        me = self.pos[half]
-        ref = self.block(half, me if outgoing else lax.rem(me + n - d, n))
-        return pltpu.make_async_remote_copy(
-            src_ref=ref,
-            dst_ref=ref,
-            send_sem=self.r_send.at[half, d - 1],
-            recv_sem=self.r_recv.at[half, d - 1],
-            device_id=self.device(half, lax.rem(me + d, n)),
-            device_id_type=MESH,
-        )
-
-    def start_direct(self):
-        for half in (0, 1):
-            for d in range(1, self.size[half]):
-                copy = self.direct_copy(half, d, True)
-                copy.start()
-                self.sent.append(copy)
-
-    def wait_direct(self):
-        for half in (0, 1):
-            for d in range(1, self.size[half]):
-                self.direct_copy(half, d, False).wait_recv()
-
     def pass_on(self, s, each=None):
         for half in (0, 1):
             for way in (0, 1):
@@ -161,95 +136,113 @@
             copy.wait_send()
 
 
-IN_HBM = (
-    "tokens",
-    "latent_down",
-    "rope_down",
-    "query_up",
-    "key_up",
-    "value_up",
-    "conv_taps",
-)
-SHARDS = ("query_down", "glu_value", "glu_gate", "head_proj", "channel_proj")
-GAINS = ("norm_gain", "query_gain", "latent_gain", "group_gain", "inv_freq")
-SCRATCH = (
-    "normed4",
-    "query_w",
-    "glu_w",
-    "keys_all",
-    "out_all",
-    "ql_send",
-    "ql_recv",
-    "gated",
-    "wide",
-    "conv_send",
-    "conv_recv",
-    "queries",
-    "row_max",
-    "row_sum",
-    "acc",
-    "head_out",
-    "part_send",
-)
-SEMS = (
-    "load_sem",
-    "shard_sem",
-    "qw_ps",
-    "qw_pr",
-    "qw_rs",
-    "qw_rr",
-    "glu_ps",
-    "glu_pr",
-    "glu_rs",
-    "glu_rr",
-    "keys_ps",
-    "keys_pr",
-    "keys_rs",
-    "keys_rr",
-    "out_ps",
-    "out_pr",
-    "out_rs",
-    "out_rr",
-    "pair_send",
-    "pair_recv",
-    "pair0_send",
-    "pair0_recv",
-    "x_send",
-    "x_recv",
-    "xp_send",
-    "xp_recv",
-    "ql_ssem",
-    "ql_rsem",
-    "cv_ssem",
-    "cv_rsem",
-    "halo_ssem",
-    "halo_rsem",
-    "fin_sem",
-)
-OUTS = ("kept", "part_recv", "log_weight")
-
-
-def kernel(nz, ny, *refs):
-    names = IN_HBM + SHARDS + GAINS + OUTS + SCRATCH + tuple("v_" + n for n in IN_HBM) + SEMS
-    r = dict(zip(names, refs, strict=True))
-    body(nz, ny, r)
-
-
-def body(nz, ny, r):
+def kernel(
+    nz,
+    ny,
+    tokens_hbm,
+    latent_down_hbm,
+    rope_down_hbm,
+    query_up_hbm,
+    key_up_hbm,
+    value_up_hbm,
+    conv_taps_hbm,
+    query_down,
+    glu_value,
+    glu_gate,
+    head_proj,
+    channel_proj,
+    norm_gain,
+    query_gain,
+    latent_gain,
+    group_gain,
+    inv_freq,
+    kept,
+    part_recv,
+    log_weight,
+    normed4,
+    query_w,
+    glu_w,
+    ch_all,
+    keys_all,
+    out_all,
+    ql_send,
+    ql_recv,
+    gated,
+    wide,
+    conv_send,
+    conv_recv,
+    queries,
+    row_max,
+    row_sum,
+    acc,
+    head_out,
+    part_send,
+    tokens,
+    latent_down,
+    rope_down,
+    query_up,
+    key_up,
+    value_up,
+    conv_taps,
+    load_sem,
+    shard_sem,
+    qw_ps,
+    qw_pr,
+    qw_rs,
+    qw_rr,
+    glu_ps,
+    glu_pr,
+    glu_rs,
+    glu_rr,
+    ch_ps,
+    ch_pr,
+    ch_rs,
+    ch_rr,
+    keys_ps,
+    keys_pr,
+    keys_rs,
+    keys_rr,
+    out_ps,
+    out_pr,
+    out_rs,
+    out_rr,
+    qp_send,
+    qp_recv,
+    chx_send,
+    chx_recv,
+    chx0_send,
+    chx0_recv,
+    chr_send,
+    chr_recv,
+    chr0_send,
+    chr0_recv,
+    pair_send,
+    pair_recv,
+    pair0_send,
+    pair0_recv,
+    x_send,
+    x_recv,
+    xp_send,
+    xp_recv,
+    ql_ssem,
+    ql_rsem,
+    cv_ssem,
+    cv_rsem,
+    halo_ssem,
+    halo_rsem,
+    fin_sem,
+):
     sp = lax.axis_index("sp")
     x = lax.axis_index("fs")
     c = lax.axis_index("tp")
     z, y = sp // ny, lax.rem(sp, ny)
     other = 1 - c
-    tokens, latent_down, rope_down = r["v_tokens"], r["v_latent_down"], r["v_rope_down"]
-    query_up, key_up, value_up, conv_taps = (r["v_" + n] for n in ("query_up", "key_up", "value_up", "conv_taps"))
-    normed4, keys_all, out_all, gated, wide = (r[n] for n in ("normed4", "keys_all", "out_all", "gated", "wide"))
-    query_w, glu_w, queries = r["query_w"], r["glu_w"], r["queries"]
-    row_max, row_sum, acc = r["row_max"], r["row_sum"], r["acc"]
     count, depth = tokens.shape
     half_rows = count // 2
     heads = key_up.shape[1] // NOPE
     partner = {"tp": other}
+    turn = 1 - 2 * c
+    behind, ahead, far = lax.rem(x - turn + NX, NX), lax.rem(x + turn + NX, NX), lax.rem(x + 2, NX)
 
     barrier = pltpu.get_barrier_semaphore()
 
@@ -274,31 +267,39 @@
     def _():
         greet(sp=sp + 1)
 
-    loads = {}
-    for k, name in enumerate(IN_HBM):
-        loads[name] = pltpu.make_async_copy(r[name], r["v_" + name], r["load_sem"].at[k])
-        loads[name].start()
-        if k == 0:
-            columns = pl.ds(pl.multiple_of(x * GROUP, GROUP), GROUP)
-            slot = (z, y)
-            wide_out = r["head_proj"].shape[-1]
-            shards = (
-                (r["query_down"].at[:, :, columns], query_w.at[slot]),
-                (r["glu_value"].at[:, :, columns], glu_w.at[z, y, :, :, pl.ds(0, GROUP)]),
-                (r["glu_gate"].at[:, :, columns], glu_w.at[z, y, :, :, pl.ds(GROUP, GROUP)]),
-                (r["head_proj"], out_all.at[z, y, :, :, pl.ds(0, wide_out)]),
-                (r["channel_proj"], out_all.at[z, y, :, :, pl.ds(wide_out, wide_out)]),
-            )
-            shards = [pltpu.make_async_copy(a, b, r["shard_sem"].at[i]) for i, (a, b) in enumerate(shards)]
-            for copy in shards:
-                copy.start()
-
-    g_query = Gather(query_w, nz, ny, z, y, r["qw_ps"], r["qw_pr"], r["qw_rs"], r["qw_rr"])
-    g_glu = Gather(glu_w, nz, ny, z, y, r["glu_ps"], r["glu_pr"], r["glu_rs"], r["glu_rr"])
-    keys_sems = (r["keys_ps"], r["keys_pr"], r["keys_rs"], r["keys_rr"])
-    g_keys = Gather(keys_all.at[c], nz, ny, z, y, *keys_sems)
-    other_keys = Gather(keys_all.at[other], nz, ny, z, y, *keys_sems)
-    g_out = Gather(out_all, nz, ny, z, y, r["out_ps"], r["out_pr"], r["out_rs"], r["out_rr"])
+    first_core = c == 0
+    a_pos, b_pos = jnp.where(first_core, z, y), jnp.where(first_core, y, z)
+    columns = pl.ds(pl.multiple_of(x * GROUP, GROUP), GROUP)
+    slots = (
+        (query_down.at[c, :, columns], query_w.at[c, a_pos, b_pos]),
+        (glu_value.at[:, :, columns], glu_w.at[z, y, :, :, pl.ds(0, GROUP)]),
+        (glu_gate.at[:, :, columns], glu_w.at[z, y, :, :, pl.ds(GROUP, GROUP)]),
+        (channel_proj.at[:, :, columns], ch_all.at[x, z, y]),
+        (head_proj, out_all.at[z, y]),
+    )
+    wanted = (
+        (tokens_hbm, tokens),
+        (latent_down_hbm, latent_down),
+        (rope_down_hbm, rope_down),
+        (query_up_hbm, query_up),
+        (key_up_hbm, key_up),
+        (value_up_hbm, value_up),
+        (conv_taps_hbm, conv_taps),
+    )
+    loads = [pltpu.make_async_copy(a, b, load_sem.at[k]) for k, (a, b) in enumerate(wanted)]
+    shards = [pltpu.make_async_copy(a, b, shard_sem.at[k]) for k, (a, b) in enumerate(slots)]
+    for copy in loads[:1] + shards + loads[1:]:
+        copy.start()
+
+    g_glu = Gather(glu_w, nz, ny, z, y, glu_ps, glu_pr, glu_rs, glu_rr)
+    g_ch = Gather(ch_all.at[x], nz, ny, z, y, ch_ps, ch_pr, ch_rs, ch_rr)
+    g_keys = Gather(keys_all.at[c], nz, ny, z, y, keys_ps, keys_pr, keys_rs, keys_rr)
+    g_out = Gather(out_all, nz, ny, z, y, out_ps, out_pr, out_rs, out_rr)
+
+    def same_places(view):
+        return Gather(view, nz, ny, z, y, keys_ps, keys_pr, keys_rs, keys_rr)
+
+    other_keys = same_places(keys_all.at[other])
     sent = []
 
     def send(src, dst, ssem, rsem, where):
@@ -318,12 +319,12 @@
     place = at_row + sp * count
     grid_row = (place // GRID_W).astype(F32)
     grid_col = lax.rem(place, GRID_W).astype(F32)
-    angles = jnp.where(lax.rem(lane, ROPE // 2) < ROPE // 4, grid_row, grid_col) * r["inv_freq"][...]
+    angles = jnp.where(lax.rem(lane, ROPE // 2) < ROPE // 4, grid_row, grid_col) * inv_freq[...]
     wide[0, 0:count, 0:ROPE] = jnp.cos(angles)
     wide[1, 0:count, 0:ROPE] = jnp.sin(angles) * jnp.where(lane < ROPE // 2, -1.0, 1.0)
 
-    loads["tokens"].wait()
-    gain = r["norm_gain"][...].astype(F32)[None, :]
+    loads[0].wait()
+    gain = norm_gain[...].astype(F32)[None, :]
     chunk = 32
     for k in range(count // chunk):
         rows = tokens[k * chunk : (k + 1) * chunk, :].astype(F32)
@@ -331,10 +332,10 @@
         which, first = divmod(k * chunk, half_rows)
         normed4[x, which, first : first + chunk, :] = value
 
-    loads["latent_down"].wait()
-    loads["rope_down"].wait()
+    loads[1].wait()
+    loads[2].wait()
     own = normed4[x, c]
-    latent = rms(dot(own, latent_down[...]), r["latent_gain"][...].astype(F32)[None, :]).astype(BF16)
+    latent = rms(dot(own, latent_down[...]), latent_gain[...].astype(F32)[None, :]).astype(BF16)
     rope_key = dot_t(own, rope_down[...])
     first = pl.multiple_of(c * half_rows, half_rows)
     rope_key = rope_key * wide[0, pl.ds(first, half_rows), 0:ROPE] + swap(rope_key) * wide[
@@ -354,52 +355,108 @@
     edges = has_low.astype(jnp.int32) + has_high.astype(jnp.int32)
     pl.semaphore_wait(barrier, (ny - 1) + (nz - 1) + (NX - 1) + 1 + edges)
 
-    g_query.start_first()
+    def query_device(a, b):
+        return {"sp": jnp.where(first_core, a * ny + b, b * ny + a)}
+
+    def query_copy(phase, d, outgoing):
+        if phase == 0:
+            b = b_pos if outgoing else lax.rem(b_pos + ny - d, ny)
+            ref, where = query_w.at[c, a_pos, b], query_device(a_pos, lax.rem(b_pos + d, ny))
+            ssem, rsem = qw_ps.at[d - 1], qw_pr.at[d - 1]
+        else:
+            a = a_pos if outgoing else lax.rem(a_pos + nz - d, nz)
+            ref, where = query_w.at[c, a], query_device(lax.rem(a_pos + d, nz), b_pos)
+            ssem, rsem = qw_rs.at[d - 1], qw_rr.at[d - 1]
+        return ref, ssem, rsem, where
+
+    def query_start(phase):
+        for d in range(1, ny):
+            ref, ssem, rsem, where = query_copy(phase, d, True)
+            send(ref, ref, ssem, rsem, where)
+
+    query_start(0)
     for way in (0, 1):
         mine = normed4.at[x, c]
         where = {"fs": lax.rem(x + (1 - 2 * way) + NX, NX)}
-        send(mine, mine, r["x_send"].at[way], r["x_recv"].at[way], where)
+        send(mine, mine, x_send.at[way], x_recv.at[way], where)
+    g_glu.start_first()
+    g_ch.start_first()
     g_keys.start_first()
-    g_glu.start_first()
     g_out.start_first()
-    for name in IN_HBM[3:]:
-        loads[name].wait()
+    for copy in loads[3:]:
+        copy.wait()
 
     def pair_keys(half, way, s):
         block = g_keys.ring_block(half, way, s, False)
-        sems = r["pair_send"].at[half, way, s - 1], r["pair_recv"].at[half, way, s - 1]
-        send(block, block, *sems, partner)
-
-    g_query.wait_first()
-    g_query.start_direct()
-
-    turn = 1 - 2 * c
-    far = lax.rem(x + 2, NX)
+        send(block, block, pair_send.at[half, way, s - 1], pair_recv.at[half, way, s - 1], partner)
+
+    def sideways(block, ssem, rsem):
+        for w in (0, 1):
+            send(block, block, ssem(w), rsem(w), {"fs": lax.rem(x + (1 - 2 * w) + NX, NX)})
+
+    def share(half, way, s):
+        block = g_ch.ring_block(half, way, s, False)
+        sideways(
+            block, lambda w: chx_send.at[w, half, way, s - 1], lambda w: chx_recv.at[w, half, way, s - 1]
+        )
+
+    def relay(s):
+        plane = same_places(ch_all.at[behind])
+        where = {"fs": ahead}
+        if s == 0:
+            for half in (0, 1):
+                block = plane.block(half, y if half else z)
+                arrived(block, chx0_send.at[c, half], chx0_recv.at[c, half])
+                send(block, block, chr0_send.at[half], chr0_recv.at[half], where)
+            return
+        for half in (0, 1):
+            for way in (0, 1):
+                block = plane.ring_block(half, way, s, False)
+                arrived(block, chx_send.at[c, half, way, s - 1], chx_recv.at[c, half, way, s - 1])
+                send(block, block, chr_send.at[half, way, s - 1], chr_recv.at[half, way, s - 1], where)
+
+    for d in range(1, ny):
+        ref, ssem, rsem, where = query_copy(0, d, False)
+        arrived(ref, ssem, rsem)
+    query_start(1)
+    mine = query_w.at[c, a_pos]
+    send(mine, mine, qp_send.at[0], qp_recv.at[0], partner)
+
+    last = nz // 2
+    g_glu.wait_first()
+    g_glu.start_ring(1)
+    g_ch.wait_first()
+    g_ch.start_ring(1)
+    for half in (0, 1):
+        sideways(
+            g_ch.block(half, y if half else z), lambda w: chx0_send.at[w, half], lambda w: chx0_recv.at[w, half]
+        )
+
     for way in (0, 1):
         src = lax.rem(x - (1 - 2 * way) + NX, NX)
         piece = normed4.at[src, c]
-        arrived(piece, r["x_send"].at[way], r["x_recv"].at[way])
-        send(piece, piece, r["xp_send"].at[way], r["xp_recv"].at[way], partner)
-    onward = normed4.at[lax.rem(x - turn + NX, NX), c]
-    send(onward, onward, r["x_send"].at[2], r["x_recv"].at[2], {"fs": lax.rem(x + turn + NX, NX)})
-
-    last = nz // 2
+        arrived(piece, x_send.at[way], x_recv.at[way])
+        send(piece, piece, xp_send.at[way], xp_recv.at[way], partner)
+    onward = normed4.at[behind, c]
+    send(onward, onward, x_send.at[2], x_recv.at[2], {"fs": ahead})
+
     g_keys.wait_first()
     g_keys.start_ring(1)
-    own_block = (g_keys.block(0, z), g_keys.block(1, y))
     for half in (0, 1):
-        send(own_block[half], own_block[half], r["pair0_send"].at[half], r["pair0_recv"].at[half], partner)
-    g_glu.wait_first()
-    g_glu.start_ring(1)
-    g_out.wait_first()
-    g_out.start_ring(1)
-
+        block = g_keys.block(half, y if half else z)
+        send(block, block, pair0_send.at[half], pair0_recv.at[half], partner)
+
+    for d in range(1, nz):
+        ref, ssem, rsem, where = query_copy(1, d, False)
+        arrived(ref, ssem, rsem)
+        send(ref, ref, qp_send.at[d], qp_recv.at[d], partner)
+
+    g_glu.pass_on(1)
+    g_ch.pass_on(1, share)
+    piece = normed4.at[far, c]
+    arrived(piece, x_send.at[2], x_recv.at[2])
+    send(piece, piece, xp_send.at[2], xp_recv.at[2], partner)
     g_keys.pass_on(1, pair_keys)
-    g_glu.pass_on(1)
-    piece = normed4.at[far, c]
-    arrived(piece, r["x_send"].at[2], r["x_recv"].at[2])
-    send(piece, piece, r["xp_send"].at[2], r["xp_recv"].at[2], partner)
-    g_out.pass_on(1)
 
     def to_parts(src, dst, ssem, rsem):
         for d in range(1, NX):
@@ -410,23 +467,32 @@
         for d in range(1, NX):
             arrived(dst.at[lax.rem(x + NX - d, NX)], ssem.at[d - 1], rsem.at[d - 1])
 
-    g_query.wait_direct()
+    for d in range(nz):
+        theirs = jnp.where(first_core, y, z)
+        arrived(query_w.at[other, lax.rem(theirs + nz - d, nz)], qp_send.at[d], qp_recv.at[d])
     for k in range(3):
         src = far if k == 2 else lax.rem(x - (1 - 2 * k) + NX, NX)
-        arrived(normed4.at[src, other], r["xp_send"].at[k], r["xp_recv"].at[k])
-    ql_send, ql_recv = r["ql_send"], r["ql_recv"]
+        arrived(normed4.at[src, other], xp_send.at[k], xp_recv.at[k])
+    pieces = []
+    for row in range(nz):
+        for column in range(ny):
+            pieces += [query_w[0, row, column], query_w[1, column, row]]
     everyone = normed4[...].reshape(NX * count, depth)
-    ql_send[...] = dot(everyone, query_w[...].reshape(depth, GROUP)).reshape(NX, count, GROUP)
-    to_parts(ql_send, ql_recv, r["ql_ssem"], r["ql_rsem"])
+    ql_send[...] = dot(everyone, jnp.concatenate(pieces, axis=0)).reshape(NX, count, GROUP)
+    to_parts(ql_send, ql_recv, ql_ssem, ql_rsem)
     ql_recv[x] = ql_send[x]
 
+    relay(0)
+    g_out.wait_first()
+    g_out.start_ring(1)
+    g_glu.pass_on(2)
+    g_ch.pass_on(2, share)
     g_keys.pass_on(2, pair_keys)
-    g_glu.pass_on(2)
-    g_out.pass_on(2)
-
-    from_parts(ql_recv, r["ql_ssem"], r["ql_rsem"])
+    relay(1)
+
+    from_parts(ql_recv, ql_ssem, ql_rsem)
     latent_query = jnp.concatenate([ql_recv[k] for k in range(NX)], axis=1)
-    latent_query = rms(latent_query, r["query_gain"][...].astype(F32)[None, :]).astype(BF16)
+    latent_query = rms(latent_query, query_gain[...].astype(F32)[None, :]).astype(BF16)
     query_all = dot(latent_query, query_up[...])
     cosine = wide[0, 0:count, 0:ROPE]
     sine = wide[1, 0:count, 0:ROPE]
@@ -480,23 +546,24 @@
         for half in (0, 1):
             for way in (0, 1):
                 ref = other_keys.ring_block(half, way, s, False)
-                arrived(ref, r["pair_send"].at[half, way, s - 1], r["pair_recv"].at[half, way, s - 1])
-
+                arrived(ref, pair_send.at[half, way, s - 1], pair_recv.at[half, way, s - 1])
+
+    g_out.pass_on(1)
+    for half in (0, 1):
+        arrived(other_keys.block(half, y if half else z), pair0_send.at[half], pair0_recv.at[half])
+    lax.fori_loop(0, 1, attend, 0)
+    g_glu.pass_on(3)
+    g_ch.pass_on(3, share)
     g_keys.pass_on(3, pair_keys)
-    g_glu.pass_on(3)
-    for half in (0, 1):
-        ref = other_keys.block(half, z if half == 0 else y)
-        arrived(ref, r["pair0_send"].at[half], r["pair0_recv"].at[half])
+    relay(2)
+    g_out.pass_on(2)
     pair_arrived(1)
-    lax.fori_loop(0, 3, attend, 0)
-    g_out.pass_on(3)
-    pair_arrived(2)
-    lax.fori_loop(3, 5, attend, 0)
+    lax.fori_loop(1, 3, attend, 0)
+
+    g_glu.pass_on(4)
+    g_ch.pass_on(4, share)
     g_keys.pass_on(4, pair_keys)
-    pair_arrived(3)
-    lax.fori_loop(5, 7, attend, 0)
-
-    g_glu.pass_on(4)
+    relay(3)
     glu_weights = glu_w[...].reshape(depth, 2 * GROUP)
     for j in range(NX):
         product = dot(normed4[j].reshape(count, depth), glu_weights)
@@ -511,8 +578,8 @@
         return pltpu.make_async_remote_copy(
             src_ref=src,
             dst_ref=dst,
-            send_sem=r["halo_ssem"].at[k],
-            recv_sem=r["halo_rsem"].at[k],
+            send_sem=halo_ssem.at[k],
+            recv_sem=halo_rsem.at[k],
             device_id={"sp": sp + 1 if up else sp - 1},
             device_id_type=MESH,
         )
@@ -535,8 +602,10 @@
     def _():
         gated[:, HALO + count :, :] = edge
 
-    pair_arrived(4)
-    lax.fori_loop(7, 8, attend, 0)
+    pair_arrived(2)
+    lax.fori_loop(3, 5, attend, 0)
+    g_out.pass_on(3)
+    relay(4)
 
     @pl.when(has_low)
     def _():
@@ -546,10 +615,9 @@
     def _():
         halo_copy(False).wait_recv()
 
-    conv_send, conv_recv = r["conv_send"], r["conv_recv"]
     reach = conv_taps.shape[0] // 2
     taps = conv_taps[:, columns].astype(F32)
-    gains = r["group_gain"][...].astype(F32)[None, :]
+    gains = group_gain[...].astype(F32)[None, :]
     channel_gain = gains[:, :GROUP]
     for k in range(1, NX):
         channel_gain = jnp.where(x == k, gains[:, k * GROUP : (k + 1) * GROUP], channel_gain)
@@ -562,10 +630,14 @@
         centred = total - jnp.mean(total, axis=-1, keepdims=True)
         spread = jnp.mean(centred * centred, axis=-1, keepdims=True)
         conv_send[j] = jax.nn.silu(centred * lax.rsqrt(spread + EPS) * channel_gain).astype(BF16)
-    to_parts(conv_send, conv_recv, r["cv_ssem"], r["cv_rsem"])
+    to_parts(conv_send, conv_recv, cv_ssem, cv_rsem)
     conv_recv[x] = conv_send[x]
 
-    head_out, log_weight = r["head_out"], r["log_weight"]
+    pair_arrived(3)
+    lax.fori_loop(5, 7, attend, 0)
+    pair_arrived(4)
+    lax.fori_loop(7, 8, attend, 0)
+
     for h in range(heads):
         rows = slice(h * count, (h + 1) * count)
         attended = (acc[rows, :] / jnp.tile(row_sum[rows, :], (1, KVR // 128))).astype(BF16)
@@ -573,24 +645,43 @@
         logs = row_max[rows, :] * scale + jnp.log(row_sum[rows, :])
         log_weight[h : h + 1, :] = jnp.transpose(logs)[0:1, :]
 
-    from_parts(conv_recv, r["cv_ssem"], r["cv_rsem"])
+    from_parts(conv_recv, cv_ssem, cv_rsem)
     mixed = jnp.concatenate([head_out[...]] + [conv_recv[k] for k in range(NX)], axis=1)
     zs = nz // 2
     width = zs * ny * 2 * out_all.shape[3]
-    part_send, part_recv = r["part_send"], r["part_recv"]
     g_out.pass_on(4)
+    for plane, sems in ((ahead, (chx_send, chx_recv, chx0_send, chx0_recv)), (far, None)):
+        places = same_places(ch_all.at[plane])
+        for half in (0, 1):
+            block = places.block(half, y if half else z)
+            if sems is None:
+                arrived(block, chr0_send.at[half], chr0_recv.at[half])
+            else:
+                arrived(block, chx0_send.at[other, half], chx0_recv.at[other, half])
+            for s in range(1, last + 1):
+                for way in (0, 1):
+                    block = places.ring_block(half, way, s, False)
+                    if sems is None:
+                        arrived(block, chr_send.at[half, way, s - 1], chr_recv.at[half, way, s - 1])
+                    else:
+                        arrived(
+                            block, chx_send.at[other, half, way, s - 1], chx_recv.at[other, half, way, s - 1]
+                        )
 
     def columns_of(core):
-        return dot_t(mixed, out_all[pl.ds(core * zs, zs)].reshape(width, mixed.shape[1])).astype(BF16)
+        rows = pl.ds(core * zs, zs)
+        parts = [out_all[rows].reshape(width, heads * VDIM)]
+        parts += [ch_all[k, rows].reshape(width, GROUP) for k in range(NX)]
+        return dot_t(mixed, jnp.concatenate(parts, axis=1)).astype(BF16)
 
     part_send[...] = columns_of(other)
-    send(part_send, part_recv, r["fin_sem"].at[0], r["fin_sem"].at[1], partner)
-    r["kept"][...] = columns_of(c)
-    arrived(part_recv, r["fin_sem"].at[0], r["fin_sem"].at[1])
+    send(part_send, part_recv, fin_sem.at[0], fin_sem.at[1], partner)
+    kept[...] = columns_of(c)
+    arrived(part_recv, fin_sem.at[0], fin_sem.at[1])
 
     for copy in sent:
         copy.wait_send()
-    for gather in (g_query, g_glu, g_keys, g_out):
+    for gather in (g_glu, g_ch, g_keys, g_out):
         gather.finish()
 
     @pl.when(has_high)
@@ -629,31 +720,13 @@
         return a.reshape(2, a.shape[0] // 2, a.shape[1])
 
     freq = (BASE ** (-np.arange(ROPE // 4, dtype=np.float64) / (ROPE // 4))).astype(np.float32)
-    given = {
-        "tokens": tokens,
-        "latent_down": latent_down,
-        "rope_down": rope_down.T,
-        "query_up": query_up,
-        "key_up": key_up,
-        "value_up": value_up,
-        "conv_taps": conv_taps,
-        "query_down": halves(query_down),
-        "glu_value": halves(glu_value),
-        "glu_gate": halves(glu_gate),
-        "head_proj": halves(head_proj.T),
-        "channel_proj": halves(channel_proj.T),
-        "norm_gain": norm_gain,
-        "query_gain": query_gain,
-        "latent_gain": latent_gain,
-        "group_gain": group_gain,
-        "inv_freq": jnp.asarray(np.tile(freq, 4)[None, :]),
-    }
+    whole = (tokens, latent_down, rope_down.T, query_up, key_up, value_up, conv_taps)
+    shards = [halves(a) for a in (query_down, glu_value, glu_gate, head_proj.T, channel_proj.T)]
+    gains = (norm_gain, query_gain, latent_gain, group_gain, jnp.asarray(np.tile(freq, 4)[None, :]))
     shard = query_down.shape[0] // 2
     out_cols = head_proj.shape[1]
-    mixed = head_proj.shape[0] + channel_proj.shape[0]
     half_cols = nz * ny * out_cols // 2
-    hops = max(nz, ny) - 1
-    last = max(nz, ny) // 2
+    last = nz // 2
     dma = pltpu.SemaphoreType.DMA
     vmem = pl.BlockSpec(memory_space=pltpu.VMEM)
     hbm = pl.BlockSpec(memory_space=pltpu.HBM)
@@ -661,13 +734,14 @@
     def buf(*shape, dtype=BF16):
         return pltpu.VMEM(shape, dtype)
 
-    ring = [dma((2, hops)), dma((2, hops)), dma((2, 2, last)), dma((2, 2, last))]
+    ring = [dma((2, ny - 1)), dma((2, ny - 1)), dma((2, 2, last)), dma((2, 2, last))]
     scratch = [
         buf(NX, 2, count // 2, depth),
-        buf(nz, ny, 2, shard, GROUP),
+        buf(2, nz, ny, shard, GROUP),
         buf(nz, ny, 2, shard, 2 * GROUP),
+        buf(NX, nz, ny, 2, out_cols // 2, GROUP),
         buf(2, nz, ny, 2, count // 8, 2 * KVR + 2 * ROPE),
-        buf(nz, ny, 2, out_cols // 2, mixed),
+        buf(nz, ny, 2, out_cols // 2, heads * VDIM),
         buf(NX, count, GROUP, dtype=F32),
         buf(NX, count, GROUP, dtype=F32),
         buf(NX, count + 2 * HALO, GROUP),
@@ -680,17 +754,18 @@
         buf(heads * count, KVR, dtype=F32),
         buf(count, heads * VDIM),
         buf(count, half_cols),
-        *[buf(*given[name].shape) for name in IN_HBM],
-        dma((len(IN_HBM),)),
-        dma((len(SHARDS),)),
-        *[dma((2, hops))] * 4,
-        *ring,
-        *ring,
-        *ring,
-        dma((2, 2, last)),
-        dma((2, 2, last)),
-        dma((2,)),
-        dma((2,)),
+        *[buf(*a.shape) for a in whole],
+        dma((len(whole),)),
+        dma((5,)),
+        *[dma((ny - 1,))] * 4,
+        *ring * 4,
+        *[dma((nz,))] * 2,
+        *[dma((2, 2, 2, last))] * 2,
+        *[dma((2, 2))] * 2,
+        *[dma((2, 2, last))] * 2,
+        *[dma((2,))] * 2,
+        *[dma((2, 2, last))] * 2,
+        *[dma((2,))] * 2,
         *[dma((3,))] * 8,
         *[dma((2,))] * 3,
     ]
@@ -701,13 +776,13 @@
             jax.ShapeDtypeStruct((count, half_cols), BF16),
             jax.ShapeDtypeStruct((heads, count), F32),
         ),
-        in_specs=[hbm] * (len(IN_HBM) + len(SHARDS)) + [vmem] * len(GAINS),
+        in_specs=[hbm] * (len(whole) + len(shards)) + [vmem] * len(gains),
         out_specs=(vmem, vmem, vmem),
         scratch_shapes=scratch,
         compiler_params=pltpu.CompilerParams(
             collective_id=0, has_side_effects=True, vmem_limit_bytes=60 * 1024 * 1024
         ),
-    )(*[given[name] for name in IN_HBM + SHARDS + GAINS])
+    )(*whole, *shards, *gains)
     return (kept.astype(F32) + came.astype(F32)).astype(BF16), log_weight
 
 

time: 91.9 us -> 78.6 us (0.86)
  Pallas kernels: 88.7 us -> 75.4 us
    pallas_call x1, Pallas kernels: 88.7 us -> 75.4 us  [per_device(): pl.pallas_call(functools.partial(kernel, nz, ny), out_shape=(jax.ShapeDty...]
where the time goes in v3:
time: 78.6 us; the launch traced here: 78.4 us
  Pallas kernels  75.4 us (96%)
  other arithmetic  1.8 us (2%)
    pallas_call x1, Pallas kernels, per_device(): pl.pallas_call(functools.partial(kernel, nz, ny), out_shape=(jax.ShapeDty...  75.4 us
    convert_element_type x1, other arithmetic, per_device(): return ((kept.astype(F32) + came.astype(F32)).astype(BF16), log_weight)  1.8 us

profile of v3, /device:TPU:1, one launch (start us, length us, event | category | flops | bytes accessed | tf_op | source)
XLA Modules:
  0.0 78.4 jit_solution(13681517696376668883)
XLA Ops:
  0.6 75.4 %shard_map.176 = (bf16[128,1024]{1,0:T(8,128)(2,1)}, bf16[128,1024]{1,0:T(8,128)(2,1)}, f32[4,128]{1,0:T(4,128)}) custom-call(bf16[128,2048]{1,0:T(8,128)(2,1)} %tokens_hbm.1, bf16[2048,256]{1,0:T(8,128)(2,1)} %latent_down_hbm.1, bf16[64,2048]{1,0:T(8,128)(2,1)} %bitcast.10, bf16[512,768]{1,0:T(8,128)(2,1)} %query_up_hbm.1, bf16[256,512]{1,0:T(8,128)(2,1)} %key_up_hbm.1, ...), custom_call_target="tpu_custom_call" | custom-call | tf_op jit(solution)/shard_map/pallas_call | solution.py:772
  76.0 0.0 copy-start
  76.0 1.8 %add_convert_fusion = bf16[128,1024]{1,0:T(8,128)(2,1)} fusion(bf16[128,1024]{1,0:T(8,128)(2,1)} %get-tuple-element.6, bf16[128,1024]{1,0:T(8,128)(2,1)} %get-tuple-element.5), kind=kLoop, calls=%fused_computation | loop fusion | flops 524288 | bytes 786432 | tf_op jit(solution)/shard_map/convert_element_type | solution.py:786
  77.8 0.0 copy-done
  77.8 0.6 copy.20
Async XLA Ops:
  76.0 1.8 %copy-start = (f32[4,128]{1,0:T(4,128)S(1)}, f32[4,128]{1,0:T(4,128)}, u32[]{:S(2)}) copy-start(f32[4,128]{1,0:T(4,128)} %get-tuple-element.11) | copy-start | bytes 6148

commit v4 on v3

v4 whole, which is shorter than its diff:
```python
import functools
import math

import jax
import jax.numpy as jnp
import numpy as np
from jax import lax
from jax.experimental import pallas as pl
from jax.experimental.pallas import tpu as pltpu
from jax.sharding import PartitionSpec as P

NOPE = 128
ROPE = 64
VDIM = 128
KVR = 256
GROUP = 128
GRID_W = 64
EPS = 1e-06
BASE = 10000.0
HALO = 16
NX = 4
F32 = jnp.float32
BF16 = jnp.bfloat16
MESH = pl.DeviceIdType.MESH


def dot(a, b):
    return jnp.dot(a, b, preferred_element_type=F32)


def dot_t(a, b):
    return lax.dot_general(a, b, (((1,), (1,)), ((), ())), preferred_element_type=F32)


def rms(values, gain):
    inv = lax.rsqrt(jnp.mean(values * values, axis=-1, keepdims=True) + EPS)
    return values * inv * gain


def swap(v):
    half = v.shape[-1] // 2
    return jnp.concatenate([v[:, half:], v[:, :half]], axis=-1)


def await_bytes(ref, sem):
    pltpu.make_async_remote_copy(
        src_ref=ref,
        dst_ref=ref,
        send_sem=sem,
        recv_sem=sem,
        device_id={"tp": 1 - lax.axis_index("tp")},
        device_id_type=MESH,
    ).wait_recv()


class Gather:
    def __init__(self, view, nz, ny, z, y, sems, steps):
        self.view, self.size, self.pos = view, (nz, ny), (z, y)
        self.sems, self.steps = sems, steps

    def device(self, axis, k):
        z, y = (k, self.pos[1]) if axis == 0 else (self.pos[0], k)
        return {"sp": z * self.size[1] + y}

    def send(self, ref, k, arrival, where):
        pltpu.make_async_remote_copy(
            src_ref=ref,
            dst_ref=ref,
            send_sem=self.sems.at[k],
            recv_sem=arrival,
            device_id=where,
            device_id_type=MESH,
        ).start()

    def start_first(self):
        z, y = self.pos
        for half in (0, 1):
            axis = 1 - half
            n = self.size[axis]
            for d in range(1, n):
                where = self.device(axis, lax.rem(self.pos[axis] + d, n))
                self.send(self.view.at[z, y, half], 0, self.sems.at[1], where)

    def wait_first(self):
        await_bytes(self.view.at[0, pl.ds(0, self.size[1] - 1)], self.sems.at[1])

    def block(self, half, k, part=None):
        n = self.size[1 - half]
        rows = slice(None) if part is None else pl.ds(part * (n // 2), n // 2)
        return self.view.at[k, rows, 0] if half == 0 else self.view.at[rows, k, 1]

    def ring_block(self, half, way, s, outgoing=False):
        n = self.size[half]
        back = s - 1 if outgoing else s
        k = lax.rem(self.pos[half] - (1 - 2 * way) * back + n, n)
        return self.block(half, k, way if s == n // 2 else None)

    def blocks(self, s):
        if s == 0:
            return [self.block(0, self.pos[0]), self.block(1, self.pos[1])]
        return [self.ring_block(half, way, s) for half in (0, 1) for way in (0, 1)]

    def like(self, s):
        return self.view.at[0] if s in (0, self.size[0] // 2) else self.view.at[pl.ds(0, 2)]

    def start_ring(self, s):
        for half in (0, 1):
            n = self.size[half]
            for way in (0, 1):
                where = self.device(half, lax.rem(self.pos[half] + (1 - 2 * way) + n, n))
                self.send(self.ring_block(half, way, s, True), 2, self.steps.at[s], where)

    def pass_on(self, s, each=None):
        await_bytes(self.like(s), self.steps.at[s])
        if s < self.size[0] // 2:
            self.start_ring(s + 1)
        if each is not None:
            each(s)

    def finish(self):
        n = self.size[0]
        await_bytes(self.view.at[0, pl.ds(0, n - 1)], self.sems.at[0])
        await_bytes(self.view.at[pl.ds(0, n - 1)], self.sems.at[2])


def kernel(
    nz,
    ny,
    tokens_hbm,
    latent_down_hbm,
    rope_down_hbm,
    query_up_hbm,
    key_up_hbm,
    value_up_hbm,
    conv_taps_hbm,
    query_down,
    glu_value,
    glu_gate,
    head_proj,
    channel_proj,
    norm_gain_hbm,
    query_gain_hbm,
    latent_gain_hbm,
    group_gain_hbm,
    inv_freq_hbm,
    kept,
    part_recv,
    log_weight,
    normed4,
    query_w,
    glu_w,
    ch_all,
    keys_all,
    out_all,
    ql_send,
    ql_recv,
    gated,
    wide,
    conv_send,
    conv_recv,
    queries,
    row_max,
    row_sum,
    acc,
    head_out,
    part_send,
    tokens,
    latent_down,
    rope_down,
    query_up,
    key_up,
    value_up,
    conv_taps,
    norm_gain,
    query_gain,
    latent_gain,
    group_gain,
    inv_freq,
    load_sem,
    shard_sem,
    query_sem,
    glu_sems,
    glu_steps,
    ch_sems,
    ch_steps,
    keys_sems,
    keys_steps,
    out_sems,
    out_steps,
    side_send,
    side_recv,
    relay_send,
    relay_recv,
    pair_send,
    pair_recv,
    x_send,
    x_recv,
    xp_send,
    xp_recv,
    ql_sem,
    cv_sem,
    halo_ssem,
    halo_rsem,
    fin_sem,
):
    sp = lax.axis_index("sp")
    x = lax.axis_index("fs")
    c = lax.axis_index("tp")
    z, y = sp // ny, lax.rem(sp, ny)
    other = 1 - c
    count, depth = tokens.shape
    half_rows = count // 2
    heads = key_up.shape[1] // NOPE
    partner = {"tp": other}
    turn = 1 - 2 * c
    behind, ahead, far = lax.rem(x - turn + NX, NX), lax.rem(x + turn + NX, NX), lax.rem(x + 2, NX)

    barrier = pltpu.get_barrier_semaphore()

    def greet(**where):
        pl.semaphore_signal(barrier, inc=1, device_id=where, device_id_type=MESH)

    for d in range(1, ny):
        greet(sp=z * ny + lax.rem(y + d, ny))
    for d in range(1, nz):
        greet(sp=lax.rem(z + d, nz) * ny + y)
    for d in range(1, NX):
        greet(fs=lax.rem(x + d, NX))
    greet(tp=other)
    has_low = sp > 0
    has_high = sp < nz * ny - 1

    @pl.when(has_low)
    def _():
        greet(sp=sp - 1)

    @pl.when(has_high)
    def _():
        greet(sp=sp + 1)

    first_core = c == 0
    a_pos, b_pos = jnp.where(first_core, z, y), jnp.where(first_core, y, z)
    columns = pl.ds(pl.multiple_of(x * GROUP, GROUP), GROUP)
    slots = (
        (query_down.at[c, :, columns], query_w.at[c, a_pos, b_pos]),
        (glu_value.at[:, :, columns], glu_w.at[z, y, :, :, pl.ds(0, GROUP)]),
        (glu_gate.at[:, :, columns], glu_w.at[z, y, :, :, pl.ds(GROUP, GROUP)]),
        (channel_proj.at[:, :, columns], ch_all.at[x, z, y]),
        (head_proj, out_all.at[z, y]),
    )
    wanted = (
        (tokens_hbm, tokens),
        (latent_down_hbm, latent_down),
        (rope_down_hbm, rope_down),
        (query_up_hbm, query_up),
        (key_up_hbm, key_up),
        (value_up_hbm, value_up),
        (conv_taps_hbm, conv_taps),
        (norm_gain_hbm, norm_gain),
        (query_gain_hbm, query_gain),
        (latent_gain_hbm, latent_gain),
        (group_gain_hbm, group_gain),
        (inv_freq_hbm, inv_freq),
    )
    loads = [pltpu.make_async_copy(a, b, load_sem.at[k]) for k, (a, b) in enumerate(wanted)]
    shards = [pltpu.make_async_copy(a, b, shard_sem.at[k]) for k, (a, b) in enumerate(slots)]
    for copy in shards + loads:
        copy.start()

    g_glu = Gather(glu_w, nz, ny, z, y, glu_sems, glu_steps)
    g_ch = Gather(ch_all.at[x], nz, ny, z, y, ch_sems, ch_steps)
    g_keys = Gather(keys_all.at[c], nz, ny, z, y, keys_sems, keys_steps)
    g_out = Gather(out_all, nz, ny, z, y, out_sems, out_steps)
    sent = []

    def send(src, dst, ssem, rsem, where):
        copy = pltpu.make_async_remote_copy(
            src_ref=src, dst_ref=dst, send_sem=ssem, recv_sem=rsem, device_id=where, device_id_type=MESH
        )
        copy.start()
        return copy

    def arrived(dst, ssem, rsem):
        pltpu.make_async_remote_copy(
            src_ref=dst, dst_ref=dst, send_sem=ssem, recv_sem=rsem, device_id=partner, device_id_type=MESH
        ).wait_recv()

    for copy in shards:
        copy.wait()
    edges = has_low.astype(jnp.int32) + has_high.astype(jnp.int32)
    pl.semaphore_wait(barrier, (ny - 1) + (nz - 1) + (NX - 1) + 1 + edges)

    def query_start(phase):
        for d in range(1, ny):
            if phase == 0:
                a, b = a_pos, lax.rem(b_pos + d, ny)
                ref = query_w.at[c, a_pos, b_pos]
            else:
                a, b = lax.rem(a_pos + d, nz), b_pos
                ref = query_w.at[c, a_pos]
            where = {"sp": jnp.where(first_core, a * ny + b, b * ny + a)}
            send(ref, ref, query_sem.at[2 * phase], query_sem.at[2 * phase + 1], where)

    query_start(0)
    g_glu.start_first()
    g_ch.start_first()
    loads[0].wait()
    loads[7].wait()
    gain = norm_gain[...].astype(F32)[None, :]
    chunk = 32
    for k in range(count // chunk):
        rows = tokens[k * chunk : (k + 1) * chunk, :].astype(F32)
        value = rms(rows, gain).astype(BF16)
        which, first = divmod(k * chunk, half_rows)
        normed4[x, which, first : first + chunk, :] = value

    for way in (0, 1):
        mine = normed4.at[x, c]
        where = {"fs": lax.rem(x + (1 - 2 * way) + NX, NX)}
        sent.append(send(mine, mine, x_send.at[way], x_recv.at[way], where))
    at_row = lax.broadcasted_iota(jnp.int32, (count, ROPE), 0)
    lane = lax.broadcasted_iota(jnp.int32, (count, ROPE), 1)
    place = at_row + sp * count
    grid_row = (place // GRID_W).astype(F32)
    grid_col = lax.rem(place, GRID_W).astype(F32)
    loads[11].wait()
    angles = jnp.where(lax.rem(lane, ROPE // 2) < ROPE // 4, grid_row, grid_col) * inv_freq[...]
    wide[0, 0:count, 0:ROPE] = jnp.cos(angles)
    wide[1, 0:count, 0:ROPE] = jnp.sin(angles) * jnp.where(lane < ROPE // 2, -1.0, 1.0)

    loads[1].wait()
    loads[2].wait()
    loads[9].wait()
    own = normed4[x, c]
    latent = rms(dot(own, latent_down[...]), latent_gain[...].astype(F32)[None, :]).astype(BF16)
    rope_key = dot_t(own, rope_down[...])
    first = pl.multiple_of(c * half_rows, half_rows)
    rope_key = rope_key * wide[0, pl.ds(first, half_rows), 0:ROPE] + swap(rope_key) * wide[
        1, pl.ds(first, half_rows), 0:ROPE
    ]
    quarter = half_rows // 2
    rope_pair = jnp.concatenate([rope_key[:quarter], rope_key[quarter:]], axis=1).astype(BF16)
    for h in (0, 1):
        lo = h * (quarter // 2)
        hi = lo + quarter // 2
        keys_all[c, z, y, h, :, 0:KVR] = latent[lo:hi]
        keys_all[c, z, y, h, :, KVR : 2 * KVR] = latent[quarter + lo : quarter + hi]
        keys_all[c, z, y, h, :, 2 * KVR :] = rope_pair[lo:hi]

    g_keys.start_first()
    g_out.start_first()
    for copy in loads[3:7] + [loads[8], loads[10]]:
        copy.wait()

    def pair_keys(s):
        for block in g_keys.blocks(s):
            send(block, block, pair_send.at[0], pair_recv.at[s], partner)

    def pair_arrived(s):
        await_bytes(g_keys.like(s), pair_recv.at[s])

    def share(s):
        for block in g_ch.blocks(s):
            for w in (0, 1):
                where = {"fs": lax.rem(x + (1 - 2 * w) + NX, NX)}
                send(block, block, side_send.at[0], side_recv.at[w, s], where)

    passing = Gather(ch_all.at[behind], nz, ny, z, y, ch_sems, ch_steps)

    def relay(s):
        await_bytes(g_ch.like(s), side_recv.at[c, s])
        for block in passing.blocks(s):
            send(block, block, relay_send.at[0], relay_recv.at[s], {"fs": ahead})

    await_bytes(query_w.at[0, 0, pl.ds(0, ny - 1)], query_sem.at[1])
    query_start(1)

    last = nz // 2
    g_glu.wait_first()
    g_glu.start_ring(1)
    g_ch.wait_first()
    g_ch.start_ring(1)

    for way in (0, 1):
        src = lax.rem(x - (1 - 2 * way) + NX, NX)
        piece = normed4.at[src, c]
        arrived(piece, x_send.at[way], x_recv.at[way])
        sent.append(send(piece, piece, xp_send.at[way], xp_recv.at[way], partner))
    onward = normed4.at[behind, c]
    sent.append(send(onward, onward, x_send.at[2], x_recv.at[2], {"fs": ahead}))

    g_keys.wait_first()
    g_keys.start_ring(1)
    pair_keys(0)

    g_out.wait_first()
    g_out.start_ring(1)

    await_bytes(query_w.at[0, pl.ds(0, nz - 1)], query_sem.at[3])
    sent.append(send(query_w.at[c], query_w.at[c], query_sem.at[4], query_sem.at[5], partner))
    piece = normed4.at[far, c]
    arrived(piece, x_send.at[2], x_recv.at[2])
    sent.append(send(piece, piece, xp_send.at[2], xp_recv.at[2], partner))
    g_glu.pass_on(1)
    g_ch.pass_on(1)

    def to_parts(src, dst, sems):
        for d in range(1, NX):
            part = lax.rem(x + d, NX)
            send(src.at[part], dst.at[x], sems.at[0], sems.at[1], {"fs": part})

    def from_parts(dst, sems):
        await_bytes(dst.at[pl.ds(0, NX - 1)], sems.at[1])

    await_bytes(query_w.at[other], query_sem.at[5])
    for k in range(3):
        src = far if k == 2 else lax.rem(x - (1 - 2 * k) + NX, NX)
        arrived(normed4.at[src, other], xp_send.at[k], xp_recv.at[k])
    pieces = []
    for row in range(nz):
        for column in range(ny):
            pieces += [query_w[0, row, column], query_w[1, column, row]]
    everyone = normed4[...].reshape(NX * count, depth)
    ql_send[...] = dot(everyone, jnp.concatenate(pieces, axis=0)).reshape(NX, count, GROUP)
    to_parts(ql_send, ql_recv, ql_sem)
    ql_recv[x] = ql_send[x]
    share(0)
    share(1)

    g_keys.pass_on(1, pair_keys)

    from_parts(ql_recv, ql_sem)
    latent_query = jnp.concatenate([ql_recv[k] for k in range(NX)], axis=1)
    latent_query = rms(latent_query, query_gain[...].astype(F32)[None, :]).astype(BF16)
    query_all = dot(latent_query, query_up[...])
    cosine = wide[0, 0:count, 0:ROPE]
    sine = wide[1, 0:count, 0:ROPE]
    nothing = jnp.zeros((count, ROPE), F32)
    for h in range(heads):
        start = h * (NOPE + ROPE)
        plain = query_all[:, start : start + NOPE].astype(BF16)
        turned = query_all[:, start + NOPE : start + NOPE + ROPE]
        turned = turned * cosine + swap(turned) * sine
        absorbed = dot_t(plain, key_up[:, h * NOPE : (h + 1) * NOPE]).astype(BF16)
        rows = slice(h * count, (h + 1) * count)
        queries[0, rows, 0:KVR] = absorbed
        queries[1, rows, 0:KVR] = absorbed
        queries[0, rows, KVR:] = jnp.concatenate([turned, nothing], axis=1).astype(BF16)
        queries[1, rows, KVR:] = jnp.concatenate([nothing, turned], axis=1).astype(BF16)

    scale = (NOPE + ROPE) ** (-0.5)
    factor = scale * math.log2(math.e)
    row_max[...] = jnp.full(row_max.shape, -1e30, F32)
    row_sum[...] = jnp.zeros(row_sum.shape, F32)
    acc[...] = jnp.zeros(acc.shape, F32)
    lines = quarter // 2

    def attend(k, carry):
        odd = lax.rem(k, 2)
        step = odd * (lax.div(k, 2) + 1) - (1 - odd) * lax.div(k, 2)
        row = lax.rem(z + step + nz, nz)
        column = lax.rem(y + step + ny, ny)
        pieces, values = [], []
        for core in (0, 1):
            upper = keys_all[core, row, :, 0].reshape(ny * lines, 2 * KVR + 2 * ROPE)
            lower = keys_all[core, :, column, 1].reshape(nz * lines, 2 * KVR + 2 * ROPE)
            block = jnp.concatenate([upper, lower], axis=0)
            tail = block[:, 2 * KVR :]
            for low in (0, 1):
                value = block[:, low * KVR : (low + 1) * KVR]
                pieces.append(dot_t(queries[low], jnp.concatenate([value, tail], axis=1)))
                values.append(value)
        scores = jnp.concatenate(pieces, axis=1)
        before = row_max[...]
        now = jnp.maximum(before, jnp.max(scores, axis=1, keepdims=True))
        shrink = jnp.exp2((before - now) * factor)
        weights = jnp.exp2((scores - jnp.tile(now, (1, scores.shape[1] // 128))) * factor)
        row_sum[...] = row_sum[...] * shrink + jnp.sum(weights, axis=1, keepdims=True)
        row_max[...] = now
        added = dot(weights.astype(BF16), jnp.concatenate(values, axis=0))
        acc[...] = acc[...] * jnp.tile(shrink, (1, KVR // 128)) + added
        return carry

    g_glu.pass_on(2)
    g_ch.pass_on(2, share)
    g_out.pass_on(1)
    pair_arrived(0)
    lax.fori_loop(0, 1, attend, 0)
    pair_arrived(1)
    g_keys.pass_on(2, pair_keys)
    lax.fori_loop(1, 2, attend, 0)
    g_glu.pass_on(3)
    g_ch.pass_on(3, share)
    relay(0)
    relay(1)
    lax.fori_loop(2, 3, attend, 0)
    g_out.pass_on(2)
    pair_arrived(2)
    lax.fori_loop(3, 4, attend, 0)

    g_glu.pass_on(4)
    g_ch.pass_on(4, share)
    relay(2)
    glu_weights = glu_w[...].reshape(depth, 2 * GROUP)
    for j in range(NX):
        product = dot(normed4[j].reshape(count, depth), glu_weights)
        gated[j, HALO : HALO + count, :] = (product[:, :GROUP] * jax.nn.sigmoid(product[:, GROUP:])).astype(BF16)

    low_src, high_src = gated.at[:, pl.ds(HALO, HALO)], gated.at[:, pl.ds(count, HALO)]
    low_dst, high_dst = gated.at[:, pl.ds(0, HALO)], gated.at[:, pl.ds(HALO + count, HALO)]

    def halo_copy(up):
        src, dst = (high_src, low_dst) if up else (low_src, high_dst)
        k = 0 if up else 1
        return pltpu.make_async_remote_copy(
            src_ref=src,
            dst_ref=dst,
            send_sem=halo_ssem.at[k],
            recv_sem=halo_rsem.at[k],
            device_id={"sp": sp + 1 if up else sp - 1},
            device_id_type=MESH,
        )

    @pl.when(has_high)
    def _():
        halo_copy(True).start()

    @pl.when(has_low)
    def _():
        halo_copy(False).start()

    edge = jnp.zeros((NX, HALO, GROUP), BF16)

    @pl.when(jnp.logical_not(has_low))
    def _():
        gated[:, 0:HALO, :] = edge

    @pl.when(jnp.logical_not(has_high))
    def _():
        gated[:, HALO + count :, :] = edge

    g_keys.pass_on(3, pair_keys)
    lax.fori_loop(4, 5, attend, 0)
    relay(3)
    g_out.pass_on(3)

    @pl.when(has_low)
    def _():
        halo_copy(True).wait_recv()

    @pl.when(has_high)
    def _():
        halo_copy(False).wait_recv()

    reach = conv_taps.shape[0] // 2
    taps = conv_taps[:, columns].astype(F32)
    gains = group_gain[...].astype(F32)[None, :]
    channel_gain = gains[:, :GROUP]
    for k in range(1, NX):
        channel_gain = jnp.where(x == k, gains[:, k * GROUP : (k + 1) * GROUP], channel_gain)
    for j in range(NX):
        wide[j, :, :] = gated[j].astype(F32)
        total = jnp.zeros((count, GROUP), F32)
        for t in range(2 * reach + 1):
            lo = HALO - reach + t
            total = total + wide[j, lo : lo + count, :] * taps[t : t + 1, :]
        centred = total - jnp.mean(total, axis=-1, keepdims=True)
        spread = jnp.mean(centred * centred, axis=-1, keepdims=True)
        conv_send[j] = jax.nn.silu(centred * lax.rsqrt(spread + EPS) * channel_gain).astype(BF16)
    to_parts(conv_send, conv_recv, cv_sem)
    conv_recv[x] = conv_send[x]

    pair_arrived(3)
    lax.fori_loop(5, 6, attend, 0)
    g_keys.pass_on(4, pair_keys)
    relay(4)
    lax.fori_loop(6, 7, attend, 0)
    pair_arrived(4)
    lax.fori_loop(7, 8, attend, 0)

    for h in range(heads):
        rows = slice(h * count, (h + 1) * count)
        attended = (acc[rows, :] / jnp.tile(row_sum[rows, :], (1, KVR // 128))).astype(BF16)
        head_out[:, h * VDIM : (h + 1) * VDIM] = dot(attended, value_up[:, h * VDIM : (h + 1) * VDIM]).astype(BF16)
        logs = row_max[rows, :] * scale + jnp.log(row_sum[rows, :])
        log_weight[h : h + 1, :] = jnp.transpose(logs)[0:1, :]

    from_parts(conv_recv, cv_sem)
    mixed = jnp.concatenate([head_out[...]] + [conv_recv[k] for k in range(NX)], axis=1)
    zs = nz // 2
    width = zs * ny * 2 * out_all.shape[3]
    g_out.pass_on(4)
    for s in range(last + 1):
        await_bytes(g_ch.like(s), side_recv.at[other, s])
        await_bytes(g_ch.like(s), relay_recv.at[s])

    def columns_of(core):
        rows = pl.ds(core * zs, zs)
        parts = [out_all[rows].reshape(width, heads * VDIM)]
        parts += [ch_all[k, rows].reshape(width, GROUP) for k in range(NX)]
        return dot_t(mixed, jnp.concatenate(parts, axis=1)).astype(BF16)

    part_send[...] = columns_of(other)
    sent.append(send(part_send, part_recv, fin_sem.at[0], fin_sem.at[1], partner))
    kept[...] = columns_of(c)
    arrived(part_recv, fin_sem.at[0], fin_sem.at[1])

    for copy in sent:
        copy.wait_send()
    await_bytes(query_w.at[0, 0, pl.ds(0, ny - 1)], query_sem.at[0])
    await_bytes(query_w.at[0, pl.ds(0, nz - 1)], query_sem.at[2])
    await_bytes(keys_all.at[0], pair_send.at[0])
    await_bytes(ch_all.at[pl.ds(0, 2)], side_send.at[0])
    await_bytes(ch_all.at[0], relay_send.at[0])
    await_bytes(ql_send.at[pl.ds(0, NX - 1)], ql_sem.at[0])
    await_bytes(conv_send.at[pl.ds(0, NX - 1)], cv_sem.at[0])
    g_glu.finish()
    g_ch.finish()
    g_keys.finish()
    g_out.finish()

    @pl.when(has_high)
    def _():
        halo_copy(True).wait_send()

    @pl.when(has_low)
    def _():
        halo_copy(False).wait_send()


def per_device(
    nz,
    ny,
    tokens,
    norm_gain,
    query_down,
    query_gain,
    latent_down,
    latent_gain,
    rope_down,
    query_up,
    key_up,
    value_up,
    glu_value,
    glu_gate,
    conv_taps,
    group_gain,
    head_proj,
    channel_proj,
):
    count, depth = tokens.shape
    heads = key_up.shape[1] // NOPE

    def halves(a):
        return a.reshape(2, a.shape[0] // 2, a.shape[1])

    freq = (BASE ** (-np.arange(ROPE // 4, dtype=np.float64) / (ROPE // 4))).astype(np.float32)
    whole = (tokens, latent_down, rope_down.T, query_up, key_up, value_up, conv_taps)
    shards = [halves(a) for a in (query_down, glu_value, glu_gate, head_proj.T, channel_proj.T)]
    gains = (norm_gain, query_gain, latent_gain, group_gain, jnp.asarray(np.tile(freq, 4)[None, :]))
    shard = query_down.shape[0] // 2
    out_cols = head_proj.shape[1]
    half_cols = nz * ny * out_cols // 2
    last = nz // 2
    dma = pltpu.SemaphoreType.DMA
    vmem = pl.BlockSpec(memory_space=pltpu.VMEM)
    hbm = pl.BlockSpec(memory_space=pltpu.HBM)

    def buf(*shape, dtype=BF16):
        return pltpu.VMEM(shape, dtype)

    scratch = [
        buf(NX, 2, count // 2, depth),
        buf(2, nz, ny, shard, GROUP),
        buf(nz, ny, 2, shard, 2 * GROUP),
        buf(NX, nz, ny, 2, out_cols // 2, GROUP),
        buf(2, nz, ny, 2, count // 8, 2 * KVR + 2 * ROPE),
        buf(nz, ny, 2, out_cols // 2, heads * VDIM),
        buf(NX, count, GROUP, dtype=F32),
        buf(NX, count, GROUP, dtype=F32),
        buf(NX, count + 2 * HALO, GROUP),
        buf(NX, count + 2 * HALO, GROUP, dtype=F32),
        buf(NX, count, GROUP),
        buf(NX, count, GROUP),
        buf(2, heads * count, KVR + 2 * ROPE),
        buf(heads * count, 128, dtype=F32),
        buf(heads * count, 128, dtype=F32),
        buf(heads * count, KVR, dtype=F32),
        buf(count, heads * VDIM),
        buf(count, half_cols),
        *[buf(*a.shape, dtype=a.dtype) for a in whole + gains],
        dma((len(whole + gains),)),
        dma((5,)),
        dma((6,)),
        *[dma((3,)), dma((last + 1,))] * 4,
        dma((1,)),
        dma((2, last + 1)),
        dma((1,)),
        dma((last + 1,)),
        dma((1,)),
        dma((last + 1,)),
        *[dma((3,))] * 4,
        *[dma((2,))] * 5,
    ]
    kept, came, log_weight = pl.pallas_call(
        functools.partial(kernel, nz, ny),
        out_shape=(
            jax.ShapeDtypeStruct((count, half_cols), BF16),
            jax.ShapeDtypeStruct((count, half_cols), BF16),
            jax.ShapeDtypeStruct((heads, count), F32),
        ),
        in_specs=[hbm] * (len(whole) + len(shards) + len(gains)),
        out_specs=(vmem, vmem, vmem),
        scratch_shapes=scratch,
        compiler_params=pltpu.CompilerParams(
            collective_id=0, has_side_effects=True, vmem_limit_bytes=60 * 1024 * 1024
        ),
    )(*whole, *shards, *gains)
    return (kept.astype(F32) + came.astype(F32)).astype(BF16), log_weight


def solution(mesh):
    sp = mesh.shape["sp"]
    ny = math.isqrt(sp)
    nz = sp // ny
    in_specs = (
        P(("fs", "sp"), None),
        P(),
        P("sp", None),
        P(),
        P(),
        P(),
        P(),
        P(None, "tp"),
        P(None, "tp"),
        P(None, "tp"),
        P("sp", "tp"),
        P("sp", "tp"),
        P(None, "tp"),
        P("tp"),
        P("tp", "sp"),
        P("tp", "sp"),
    )
    out_specs = (P(("fs", "sp"), "tp"), P("tp", ("fs", "sp")))
    return jax.shard_map(
        functools.partial(per_device, nz, ny), mesh=mesh, in_specs=in_specs, out_specs=out_specs, check_vma=False
    )
```

time: 78.6 us -> 71.8 us (0.913)
  Pallas kernels: 75.4 us -> 68.7 us
    pallas_call x1, Pallas kernels: 75.4 us -> 68.7 us  [per_device(): pl.pallas_call(functools.partial(kernel, nz, ny), out_shape=(jax.ShapeDty...]
where the time goes in v4:
time: 71.8 us; the launch traced here: 71.7 us
  Pallas kernels  68.7 us (96%)
  other arithmetic  1.8 us (3%)
    pallas_call x1, Pallas kernels, per_device(): pl.pallas_call(functools.partial(kernel, nz, ny), out_shape=(jax.ShapeDty...  68.7 us
    convert_element_type x1, other arithmetic, per_device(): return ((kept.astype(F32) + came.astype(F32)).astype(BF16), log_weight)  1.8 us

profile of v4, /device:TPU:1, one launch (start us, length us, event | category | flops | bytes accessed | tf_op | source)
XLA Modules:
  0.0 71.7 jit_solution(13130141628498732300)
XLA Ops:
  0.6 68.7 %shard_map.176 = (bf16[128,1024]{1,0:T(8,128)(2,1)}, bf16[128,1024]{1,0:T(8,128)(2,1)}, f32[4,128]{1,0:T(4,128)}) custom-call(bf16[128,2048]{1,0:T(8,128)(2,1)} %tokens_hbm.1, bf16[2048,256]{1,0:T(8,128)(2,1)} %latent_down_hbm.1, bf16[64,2048]{1,0:T(8,128)(2,1)} %bitcast.10, bf16[512,768]{1,0:T(8,128)(2,1)} %query_up_hbm.1, bf16[256,512]{1,0:T(8,128)(2,1)} %key_up_hbm.1, ...), custom_call_target="tpu_custom_call" | custom-call | tf_op jit(solution)/shard_map/pallas_call | solution.py:705
  69.3 0.0 copy-start
  69.3 1.8 %add_convert_fusion = bf16[128,1024]{1,0:T(8,128)(2,1)} fusion(bf16[128,1024]{1,0:T(8,128)(2,1)} %get-tuple-element.6, bf16[128,1024]{1,0:T(8,128)(2,1)} %get-tuple-element.5), kind=kLoop, calls=%fused_computation | loop fusion | flops 524288 | bytes 786432 | tf_op jit(solution)/shard_map/convert_element_type | solution.py:719
  71.1 0.0 copy-done
  71.1 0.6 copy.20
Async XLA Ops:
  69.3 1.8 %copy-start = (f32[4,128]{1,0:T(4,128)S(1)}, f32[4,128]{1,0:T(4,128)}, u32[]{:S(2)}) copy-start(f32[4,128]{1,0:T(4,128)} %get-tuple-element.11) | copy-start | bytes 6148

commit v5 on v4

--- a/solution.py
+++ b/solution.py
@@ -348,7 +348,6 @@
         keys_all[c, z, y, h, :, 2 * KVR :] = rope_pair[lo:hi]
 
     g_keys.start_first()
-    g_out.start_first()
     for copy in loads[3:7] + [loads[8], loads[10]]:
         copy.wait()
 
@@ -374,6 +373,7 @@
 
     await_bytes(query_w.at[0, 0, pl.ds(0, ny - 1)], query_sem.at[1])
     query_start(1)
+    g_out.start_first()
 
     last = nz // 2
     g_glu.wait_first()
@@ -468,17 +468,20 @@
             tail = block[:, 2 * KVR :]
             for low in (0, 1):
                 value = block[:, low * KVR : (low + 1) * KVR]
-                pieces.append(dot_t(queries[low], jnp.concatenate([value, tail], axis=1)))
+                pieces.append((low, jnp.concatenate([value, tail], axis=1)))
                 values.append(value)
-        scores = jnp.concatenate(pieces, axis=1)
-        before = row_max[...]
-        now = jnp.maximum(before, jnp.max(scores, axis=1, keepdims=True))
-        shrink = jnp.exp2((before - now) * factor)
-        weights = jnp.exp2((scores - jnp.tile(now, (1, scores.shape[1] // 128))) * factor)
-        row_sum[...] = row_sum[...] * shrink + jnp.sum(weights, axis=1, keepdims=True)
-        row_max[...] = now
-        added = dot(weights.astype(BF16), jnp.concatenate(values, axis=0))
-        acc[...] = acc[...] * jnp.tile(shrink, (1, KVR // 128)) + added
+        size = row_max.shape[0] // 2
+        parts = [slice(p * size, (p + 1) * size) for p in range(2)]
+        wide_scores = [jnp.concatenate([dot_t(queries[low, rows], piece) for low, piece in pieces], axis=1) for rows in parts]
+        stacked = jnp.concatenate(values, axis=0)
+        for rows, scores in zip(parts, wide_scores):
+            before = row_max[rows]
+            now = jnp.maximum(before, jnp.max(scores, axis=1, keepdims=True))
+            shrink = jnp.exp2((before - now) * factor)
+            weights = jnp.exp2((scores - jnp.tile(now, (1, scores.shape[1] // 128))) * factor)
+            row_sum[rows] = row_sum[rows] * shrink + jnp.sum(weights, axis=1, keepdims=True)
+            row_max[rows] = now
+            acc[rows] = acc[rows] * jnp.tile(shrink, (1, KVR // 128)) + dot(weights.astype(BF16), stacked)
         return carry
 
     g_glu.pass_on(2)
@@ -496,8 +499,9 @@
     lax.fori_loop(2, 3, attend, 0)
     g_out.pass_on(2)
     pair_arrived(2)
-    lax.fori_loop(3, 4, attend, 0)
-
+    lax.fori_loop(3, 5, attend, 0)
+
+    g_keys.pass_on(3, pair_keys)
     g_glu.pass_on(4)
     g_ch.pass_on(4, share)
     relay(2)
@@ -539,9 +543,9 @@
     def _():
         gated[:, HALO + count :, :] = edge
 
-    g_keys.pass_on(3, pair_keys)
-    lax.fori_loop(4, 5, attend, 0)
     relay(3)
+    pair_arrived(3)
+    lax.fori_loop(5, 6, attend, 0)
     g_out.pass_on(3)
 
     @pl.when(has_low)
@@ -570,8 +574,6 @@
     to_parts(conv_send, conv_recv, cv_sem)
     conv_recv[x] = conv_send[x]
 
-    pair_arrived(3)
-    lax.fori_loop(5, 6, attend, 0)
     g_keys.pass_on(4, pair_keys)
     relay(4)
     lax.fori_loop(6, 7, attend, 0)
@@ -626,6 +628,11 @@
     @pl.when(has_low)
     def _():
         halo_copy(False).wait_send()
+
+
+def add_up(kept, came, logs, out, log_weight):
+    out[...] = (kept[...].astype(F32) + came[...].astype(F32)).astype(BF16)
+    log_weight[...] = logs[...]
 
 
 def per_device(
@@ -716,7 +723,12 @@
             collective_id=0, has_side_effects=True, vmem_limit_bytes=60 * 1024 * 1024
         ),
     )(*whole, *shards, *gains)
-    return (kept.astype(F32) + came.astype(F32)).astype(BF16), log_weight
+    return pl.pallas_call(
+        add_up,
+        out_shape=(jax.ShapeDtypeStruct(kept.shape, BF16), jax.ShapeDtypeStruct(log_weight.shape, F32)),
+        in_specs=[vmem] * 3,
+        out_specs=(vmem, vmem),
+    )(kept, came, log_weight)
 
 
 def solution(mesh):

time: 71.8 us -> 70.1 us (0.976)
  other arithmetic: 1.8 us -> 0 us
    convert_element_type x1 -> x0, other arithmetic: 1.8 us -> none  [per_device(): return ((kept.astype(F32) + came.astype(F32)).astype(BF16), log_weight)]
    pallas_call x0 -> x1, Pallas kernels: none -> 1.8 us  [per_device(): pl.pallas_call(add_up, out_shape=(jax.ShapeDtypeStruct(kept.shape, BF16),...]
    pallas_call x1, Pallas kernels: 68.7 us -> 67.5 us  [per_device(): pl.pallas_call(functools.partial(kernel, nz, ny), out_shape=(jax.ShapeDty...]
where the time goes in v5:
time: 70.1 us; the launch traced here: 69.9 us
  Pallas kernels  69.3 us (99%)
    pallas_call x1, Pallas kernels, per_device(): pl.pallas_call(functools.partial(kernel, nz, ny), out_shape=(jax.ShapeDty...  67.5 us
    pallas_call x1, Pallas kernels, per_device(): pl.pallas_call(add_up, out_shape=(jax.ShapeDtypeStruct(kept.shape, BF16),...  1.8 us

profile of v5, /device:TPU:1, one launch (start us, length us, event | category | flops | bytes accessed | tf_op | source)
XLA Modules:
  0.0 69.9 jit_solution(10825020096431674169)
XLA Ops:
  0.6 67.5 %shard_map.176 = (bf16[128,1024]{1,0:T(8,128)(2,1)}, bf16[128,1024]{1,0:T(8,128)(2,1)}, f32[4,128]{1,0:T(4,128)}) custom-call(bf16[128,2048]{1,0:T(8,128)(2,1)} %tokens_hbm.1, bf16[2048,256]{1,0:T(8,128)(2,1)} %latent_down_hbm.1, bf16[64,2048]{1,0:T(8,128)(2,1)} %bitcast.10, bf16[512,768]{1,0:T(8,128)(2,1)} %query_up_hbm.1, bf16[256,512]{1,0:T(8,128)(2,1)} %key_up_hbm.1, ...), custom_call_target="tpu_custom_call" | custom-call | tf_op jit(solution)/shard_map/pallas_call | solution.py:712
  68.1 1.8 %shard_map.177 = (bf16[128,1024]{1,0:T(8,128)(2,1)}, f32[4,128]{1,0:T(4,128)}) custom-call(bf16[128,1024]{1,0:T(8,128)(2,1)} %get-tuple-element.5.kept, bf16[128,1024]{1,0:T(8,128)(2,1)} %get-tuple-element.6.came, f32[4,128]{1,0:T(4,128)} %get-tuple-element.7.logs), custom_call_target="tpu_custom_call" | custom-call | tf_op jit(solution)/shard_map/pallas_call | solution.py:726
